TPU v7x, 32 devices: a whole 2x2x4 slice. The times are simulated.
32 devices in a mesh: fs: 16 (over z, y, core), tp: 2 (over x).
Axes of the slice: x: 2, y: 2, z: 4, core: 2. Of those that a mesh axis runs over, the one named last changes fastest.
Arguments:
- saved_input: bfloat16 [8192, 3072], P('fs'), may hold values from -6 to 6
- output_cotangent: bfloat16 [8192, 3072], P('fs'), may hold values from -6 to 6
- recurrent_output: bfloat16 [8192, 1536], P('fs', 'tp'), may hold values from -6 to 6
- forget_logit: bfloat16 [8192, 1536], P('fs', 'tp'), may hold values from -12 to 12
- forget_cotangent: bfloat16 [8192, 1536], P('fs', 'tp'), may hold values from -6 to 6
- lower_bound: float32 [1536], P('tp'), may hold values from 0.2 to 0.9
- basis_in: bfloat16 [3072, 384], P('fs'), may hold values from -1.2629537 to 1.2629537
- basis_out: bfloat16 [3072, 384], P('fs'), may hold values from -1.2629537 to 1.2629537
- moment_in: float32 [384, 1536], P('fs', 'tp'), may hold values from -6 to 6
- second_in: float32 [384, 1536], P('fs', 'tp'), may hold values from 0.25 to 4
- moment_out: float32 [384, 1536], P('fs', 'tp'), may hold values from -6 to 6
- second_out: float32 [384, 1536], P('fs', 'tp'), may hold values from 0.25 to 4
- weight_in: float32 [3072, 1536], P('fs', 'tp'), may hold values from -0.109375 to 0.109375
- weight_out: float32 [1536, 3072], P('tp', 'fs'), may hold values from -0.15625 to 0.15625
Outputs:
- moment_in_new: float32 [384, 1536], P('fs', 'tp')
- second_in_new: float32 [384, 1536], P('fs', 'tp')
- moment_out_new: float32 [384, 1536], P('fs', 'tp')
- second_out_new: float32 [384, 1536], P('fs', 'tp')
- weight_in_new: float32 [3072, 1536], P('fs', 'tp')
- weight_out_new: float32 [1536, 3072], P('tp', 'fs')
- copy_in: bfloat16 [3072, 1536], P(None, 'tp')
- copy_out: bfloat16 [1536, 3072], P('tp')
All inputs are finite; a program needn't handle non-finite values.
Results may differ from a plain program's by a relative error of at most 0.0023.
Values may be sent and summed in bfloat16 or wider, within the bound.
A program may use at most 64 MiB of HBM per device.

v0:
```python
import functools

import jax
import jax.numpy as jnp
from jax import lax
from jax.experimental import pallas as pl
from jax.experimental.pallas import tpu as pltpu
from jax.sharding import PartitionSpec as P

MESH = pl.DeviceIdType.MESH
F32 = jnp.float32
BF16 = jnp.bfloat16
UNROLL = 16


def loop(start, stop, body):
    if stop - start <= UNROLL:
        for i in range(start, stop):
            body(i)
    else:

        @pl.loop(start, stop)
        def _(i):
            body(i)


def mod(value, n):
    return lax.rem(value + 2 * n, n)


def kernel(
    nf,
    nt,
    limit,
    x_hbm,
    y_hbm,
    rec_hbm,
    logit_hbm,
    fcot_hbm,
    lower_ref,
    basis_in_hbm,
    basis_out_hbm,
    m_in,
    s_in,
    m_out,
    s_out,
    w_in,
    w_out,
    mn_in,
    sn_in,
    mn_out,
    sn_out,
    wn_in,
    wn_out,
    copy_in,
    copy_out,
    x,
    y,
    rec,
    logit,
    fcot,
    bas_in,
    bas_out,
    gate,
    term,
    coded,
    part,
    peer,
    hop,
    step,
    flat,
    wb_in,
    wb_out,
    tots,
    load_sem,
    base_sem,
    send_sem,
    ring_a,
    ring_b,
    ring_d,
    ring_f,
    pair_sem,
    sum_sem,
    tot_sem,
):
    f = lax.axis_index("fs")
    tp = lax.axis_index("tp")
    n = nf // 2
    z = n // 2
    core = lax.rem(f, 2)
    chip = f // 2
    row, column = chip // 2, lax.rem(chip, 2)
    me = (1 - column) * row + column * (n - 1 - row)
    partner = (f + 1 - 2 * core, tp)

    def chip_at(position):
        side = position // z
        return 2 * ((1 - side) * position + side * (n - 1 - position)) + side

    def dev_at(position):
        return chip_at(position) * 2 + core

    loads = [
        pltpu.make_async_copy(src, dst, load_sem.at[i])
        for i, (src, dst) in enumerate(
            ((logit_hbm, logit), (fcot_hbm, fcot), (x_hbm, x), (y_hbm, y), (rec_hbm, rec))
        )
    ]
    depth = basis_in_hbm.shape[0]
    cut = 2 if depth % 32 == 0 else 1
    piece = depth // cut

    def rows(ref, dev, c):
        return ref.at[pl.ds(pl.multiple_of(dev * depth + c * piece, piece), piece)]

    def own(ref, dev):
        return ref.at[pl.ds(pl.multiple_of(dev * depth, depth), depth)]

    own_loads = [
        pltpu.make_async_copy(basis_in_hbm, own(bas_in, f), base_sem.at[0]),
        pltpu.make_async_copy(basis_out_hbm, own(bas_out, f), base_sem.at[1]),
    ]
    for copy in own_loads + loads:
        copy.start()

    barrier = pltpu.get_barrier_semaphore()
    everyone = nf * nt
    my_id = f * nt + tp

    def other(i):
        target = lax.rem(my_id + i, everyone)
        return (target // nt, lax.rem(target, nt))

    @pl.loop(1, everyone)
    def _(i):
        pl.semaphore_signal(barrier, inc=1, device_id=other(i), device_id_type=MESH)

    pl.semaphore_wait(barrier, everyone - 1)

    far = n // 2
    near = n - 1 - far
    one_way = ((0, 1, n - 1), (1, -1, n - 1))
    two_way = ((0, 1, far), (1, -1, far), (0, -1, near), (1, 1, near))

    def neighbour(way):
        return (dev_at(mod(me + way, n)), tp)

    def gather(flows, view, chunks, ring_sem, phase, between=None):
        stride = flows[0][2]

        def remote(j, s, c, sems, target):
            t, way, _ = flows[j]
            block = view(t, dev_at(mod(me - way * s, n)), c)
            return pltpu.make_async_remote_copy(
                src_ref=block,
                dst_ref=block,
                send_sem=sems[0],
                recv_sem=sems[1],
                device_id=target,
                device_id_type=MESH,
            )

        def ring_copy(j, s, c):
            sems = send_sem.at[phase, j * stride + s, c], ring_sem.at[j, s, c]
            return remote(j, s, c, sems, neighbour(flows[j][1]))

        def pair_copy(j, s, c):
            at = j * (stride + 1) + s
            sems = pair_sem.at[phase, 0, at, c], pair_sem.at[phase, 1, at, c]
            return remote(j, s, c, sems, partner)

        def each(s, act):
            for c in range(chunks):
                for j in range(len(flows)):
                    act(j, s, c)

        def move(j, s, c, first=False, last=False):
            if not first:
                ring_copy(j, s - 1, c).wait_recv()
            if not last:
                ring_copy(j, s, c).start()
            if not first or j < 2:
                pair_copy(j, s, c).start()

        least = min(hops for _, _, hops in flows)
        most = max(hops for _, _, hops in flows)
        each(0, functools.partial(move, first=True))
        if between is not None:
            between()
        loop(1, least, lambda s: each(s, move))
        for s in range(least, most + 1):
            for c in range(chunks):
                for j, (_, _, hops) in enumerate(flows):
                    if s <= hops:
                        move(j, s, c, last=s == hops)

        def finish(j, s, c):
            pair_copy(j, s, c).wait()

        def sent(j, s, c):
            ring_copy(j, s, c).wait_send()

        for c in range(chunks):
            for j, (_, _, hops) in enumerate(flows):
                if j < 2:
                    finish(j, 0, c)
                for s in range(least, hops):
                    sent(j, s, c)
                for s in range(least, hops + 1):
                    finish(j, s, c)
        loop(1, least, lambda s: each(s, finish))
        loop(0, least, lambda s: each(s, sent))

    def make_gate():
        loads[0].wait()
        loads[1].wait()
        tile = 64

        @pl.loop(0, gate.shape[0] // tile)
        def _(i):
            at = pl.ds(pl.multiple_of(i * tile, tile), tile)
            sig = jax.nn.sigmoid(logit[at].astype(F32))
            gate[at] = (
                fcot[at].astype(F32) * (1.0 - lower_ref[...]) * sig * (1.0 - sig)
            ).astype(BF16)

    for copy in own_loads:
        copy.wait()
    gather(
        one_way,
        lambda t, dev, c: rows((bas_in, bas_out)[t], dev, c),
        cut,
        ring_a,
        0,
        make_gate,
    )

    for copy in loads[2:]:
        copy.wait()
    units = gate.shape[1]
    span = part.shape[2]
    lanes = 2 if units % 256 == 0 else 1
    width = units // lanes

    def encode(data, basis):
        tile = 128

        @pl.loop(0, data.shape[0] // tile)
        def _(i):
            at = pl.ds(pl.multiple_of(i * tile, tile), tile)
            coded[at] = jnp.dot(data[at], basis[...], preferred_element_type=F32).astype(BF16)

    def project(t, cot):
        for c in range(lanes):
            at = slice(c * width, (c + 1) * width)
            term[:, at] = lax.dot_general(
                coded[...], cot[:, at], (((0,), (0,)), ((), ())), preferred_element_type=F32
            )
        for k in range(nf):
            part[t * 2 + k % 2, k // 2] = term[k * span : (k + 1) * span]

    def pair_sum(t):
        return pltpu.make_async_remote_copy(
            src_ref=part.at[t * 2 + 1 - core],
            dst_ref=peer.at[t],
            send_sem=sum_sem.at[0, t],
            recv_sem=sum_sem.at[1, t],
            device_id=partner,
            device_id_type=MESH,
        )

    def ring_add(j, s, c):
        at = pl.ds(c * width, width)
        return pltpu.make_async_remote_copy(
            src_ref=hop.at[j, s, :, at],
            dst_ref=hop.at[j, s + 1, :, at],
            send_sem=send_sem.at[3, j * far + s, c],
            recv_sem=ring_b.at[j, s, c],
            device_id=neighbour(two_way[j][1]),
            device_id_type=MESH,
        )

    def mine(j, s, c):
        t, way, hops = two_way[j]
        at = pl.ds(c * width, width)
        place = chip_at(mod(me + way * (hops - s), n))
        return part[t * 2 + core, place, :, at] + peer[t, place, :, at]

    def begin(t):
        pair_sum(t).wait_recv()
        for c in range(lanes):
            at = pl.ds(c * width, width)
            for j in (t, t + 2):
                if two_way[j][2] > 0:
                    hop[j, 0, :, at] = mine(j, 0, c)
                    ring_add(j, 0, c).start()

    def relay(j, s, c):
        at = pl.ds(c * width, width)
        ring_add(j, s - 1, c).wait_recv()
        hop[j, s, :, at] = hop[j, s, :, at] + mine(j, s, c)
        ring_add(j, s, c).start()

    def flows_do(act, s, which=range(4)):
        for c in range(lanes):
            for j in which:
                act(j, s, c)

    encode(x, bas_in)
    project(0, gate)
    pair_sum(0).start()
    encode(y, bas_out)
    begin(0)
    project(1, rec)
    pair_sum(1).start()
    begin(1)
    loop(1, near, lambda s: flows_do(relay, s))
    flows_do(relay, far - 1, range(2))
    for c in range(lanes):
        for t in range(2):
            at = pl.ds(c * width, width)
            ring_add(t + 2, near - 1, c).wait_recv()
            hop[t + 2, near, :, at] = hop[t + 2, near, :, at] + mine(t + 2, near, c)
    for c in range(lanes):
        for t in range(2):
            at = pl.ds(c * width, width)
            ring_add(t, far - 1, c).wait_recv()
            hop[t, far, :, at] = hop[t, far, :, at] + hop[t + 2, near, :, at]

    low = [hop[t, far] for t in range(2)]
    square = jnp.sum(low[0] * low[0] + low[1] * low[1], axis=(0, 1), keepdims=True)
    tots[my_id] = jnp.broadcast_to(square, tots.shape[1:])

    def tell(i):
        return pltpu.make_async_remote_copy(
            src_ref=tots.at[my_id],
            dst_ref=tots.at[my_id],
            send_sem=tot_sem.at[0],
            recv_sem=tot_sem.at[1],
            device_id=other(i),
            device_id_type=MESH,
        )

    @pl.loop(1, everyone)
    def _(i):
        tell(i).start()

    def sent_add(j, s, c):
        ring_add(j, s, c).wait_send()

    loop(0, near, lambda s: flows_do(sent_add, s))
    flows_do(sent_add, far - 1, range(2))
    for t in range(2):
        pair_sum(t).wait_send()
    all_tots = tots.at[pl.ds(0, everyone - 1)]
    pltpu.make_async_copy(all_tots, all_tots, tot_sem.at[1]).wait()
    pltpu.make_async_copy(all_tots, all_tots, tot_sem.at[0]).wait()

    total = jnp.sum(tots[...], axis=0)
    clip = jnp.minimum(1.0, jnp.sqrt(F32(limit)) * lax.rsqrt(total + 1e-06))[0:1, 0:1]
    for t, (m, s2, mn, sn) in enumerate(
        ((m_in, s_in, mn_in, sn_in), (m_out, s_out, mn_out, sn_out))
    ):
        grad = clip * hop[t, far]
        moment = 0.8 * m[...] + 0.2 * grad
        second = 0.9 * s2[...] + 0.1 * grad * grad
        mn[...] = moment
        sn[...] = second
        step[t, f] = moment / (jnp.sqrt(second) + 1e-08)

    gather(
        two_way,
        lambda t, dev, c: step.at[t, dev, :, pl.ds(c * width, width)],
        lanes,
        ring_d,
        1,
    )

    for t, (basis, w, wn, wb) in enumerate(
        ((bas_in, w_in, wn_in, wb_in), (bas_out, w_out, wn_out, wb_out))
    ):
        for k in range(nf):
            flat[k * span : (k + 1) * span] = step[t, k]
        whole = flat[...]
        high = whole.astype(BF16)
        rest = (whole - high.astype(F32)).astype(BF16)
        mat = own(basis, f)[...]
        update = jnp.dot(mat, rest, preferred_element_type=F32) + jnp.dot(
            mat, high, preferred_element_type=F32
        )
        new = w[...] - 0.01 * update
        wn[...] = new
        wb[...] = new.astype(BF16)

    puts = [
        pltpu.make_async_copy(wb_in, own(copy_in, f), base_sem.at[0]),
        pltpu.make_async_copy(wb_out, own(copy_out, f), base_sem.at[1]),
    ]
    for copy in puts:
        copy.start()
    for copy in puts:
        copy.wait()
    gather(
        one_way, lambda t, dev, c: rows((copy_in, copy_out)[t], dev, c), cut, ring_f, 2
    )


def settle(*refs):
    ins, outs = refs[:8], refs[8:]

    @pl.when(pl.program_id(0) == 0)
    def _():
        for src, dst in zip(ins[:6], outs[:6]):
            dst[...] = src[...]

    outs[6][...] = ins[6][...]
    outs[7][...] = ins[7][...].T


def body(
    saved_input,
    output_cotangent,
    recurrent_output,
    forget_logit,
    forget_cotangent,
    lower_bound,
    basis_in,
    basis_out,
    moment_in,
    second_in,
    moment_out,
    second_out,
    weight_in,
    weight_out,
):
    nf, nt = lax.axis_size("fs"), lax.axis_size("tp")
    n = nf // 2
    tokens, model = saved_input.shape
    units = recurrent_output.shape[1]
    depth, rank = basis_in.shape
    span = moment_in.shape[0]
    limit = 2.0 * rank * units * nt
    small = jax.ShapeDtypeStruct((span, units), F32)
    weight = jax.ShapeDtypeStruct((depth, units), F32)
    copied = jax.ShapeDtypeStruct((model, units), BF16)
    cut = 2 if depth % 32 == 0 else 1
    lanes = 2 if units % 256 == 0 else 1
    most = max(cut, lanes)
    hbm = pl.BlockSpec(memory_space=pl.ANY)
    vmem = pl.BlockSpec(memory_space=pltpu.VMEM)
    dma = pltpu.SemaphoreType.DMA
    outs = pl.pallas_call(
        functools.partial(kernel, nf, nt, limit),
        out_shape=(small, small, small, small, weight, weight, copied, copied),
        in_specs=[hbm] * 5 + [vmem] + [hbm] * 2 + [vmem] * 6,
        out_specs=[vmem] * 6 + [hbm] * 2,
        scratch_shapes=[
            pltpu.VMEM((tokens, model), BF16),
            pltpu.VMEM((tokens, model), BF16),
            pltpu.VMEM((tokens, units), BF16),
            pltpu.VMEM((tokens, units), BF16),
            pltpu.VMEM((tokens, units), BF16),
            pltpu.VMEM((model, rank), BF16),
            pltpu.VMEM((model, rank), BF16),
            pltpu.VMEM((tokens, units), BF16),
            pltpu.VMEM((rank, units), F32),
            pltpu.VMEM((tokens, rank), BF16),
            pltpu.VMEM((4, n, span, units), F32),
            pltpu.VMEM((2, n, span, units), F32),
            pltpu.VMEM((4, n // 2 + 1, span, units), F32),
            pltpu.VMEM((2, nf, span, units), F32),
            pltpu.VMEM((rank, units), F32),
            pltpu.VMEM((depth, units), BF16),
            pltpu.VMEM((depth, units), BF16),
            pltpu.VMEM((nf * nt, 8, 128), F32),
            dma((5,)),
            dma((2,)),
            dma((4, 2 * n, most)),
            dma((2, n - 1, cut)),
            dma((4, n // 2, lanes)),
            dma((4, n // 2 + 1, lanes)),
            dma((2, n - 1, cut)),
            dma((3, 2, 2 * n + 4, most)),
            dma((2, 2)),
            dma((2,)),
        ],
        compiler_params=pltpu.CompilerParams(
            collective_id=0, has_side_effects=True, vmem_limit_bytes=60 * 1024 * 1024
        ),
    )(
        saved_input,
        output_cotangent,
        recurrent_output,
        forget_logit,
        forget_cotangent,
        lower_bound[None, :],
        basis_in,
        basis_out,
        moment_in,
        second_in,
        moment_out,
        second_out,
        weight_in,
        weight_out.T,
    )
    blocks = 8 if model % 1024 == 0 else 1
    rows = model // blocks
    tall = pl.BlockSpec((rows, units), lambda i: (i, 0))
    kept = [pl.BlockSpec(o.shape, lambda i: (0, 0)) for o in outs[:6]]
    outs = pl.pallas_call(
        settle,
        grid=(blocks,),
        out_shape=(small, small, small, small, weight, weight, copied)
        + (jax.ShapeDtypeStruct((units, model), BF16),),
        in_specs=kept + [tall, tall],
        out_specs=kept + [tall, pl.BlockSpec((units, rows), lambda i: (0, i))],
        compiler_params=pltpu.CompilerParams(dimension_semantics=("arbitrary",)),
    )(*outs)
    return tuple(outs[:5]) + (outs[5].T, outs[6], outs[7])


def solution(mesh):
    return jax.shard_map(
        body,
        mesh=mesh,
        in_specs=(
            P("fs", None),
            P("fs", None),
            P("fs", "tp"),
            P("fs", "tp"),
            P("fs", "tp"),
            P("tp"),
            P("fs", None),
            P("fs", None),
            P("fs", "tp"),
            P("fs", "tp"),
            P("fs", "tp"),
            P("fs", "tp"),
            P("fs", "tp"),
            P("tp", "fs"),
        ),
        out_specs=(
            P("fs", "tp"),
            P("fs", "tp"),
            P("fs", "tp"),
            P("fs", "tp"),
            P("fs", "tp"),
            P("tp", "fs"),
            P(None, "tp"),
            P("tp", None),
        ),
        check_vma=False,
    )
```

profile of v0, /device:TPU:0, one launch (start us, length us, event | category | flops | bytes accessed | tf_op | source)
XLA Modules:
  0.0 149.3 jit_solution(5309802499981705465)
XLA Ops:
  0.6 1.3 broadcast_in_dim.3.lower_ref
  1.9 136.5 %shard_map.197 = (f32[24,768]{1,0:T(8,128)}, f32[24,768]{1,0:T(8,128)}, f32[24,768]{1,0:T(8,128)}, f32[24,768]{1,0:T(8,128)}, f32[192,768]{1,0:T(8,128)}, /*inde...) custom-call(bf16[512,3072]{1,0:T(8,128)(2,1)} %x_hbm.1, bf16[512,3072]{1,0:T(8,128)(2,1)} %y_hbm.1, ...), custom_call_target="tpu_custom_call" | custom-call | tf_op jit(solution)/shard_map/pallas_call | solution.py:452
  138.4 10.9 %shard_map.198 = (f32[24,768]{1,0:T(8,128)}, f32[24,768]{1,0:T(8,128)}, f32[24,768]{1,0:T(8,128)}, f32[24,768]{1,0:T(8,128)}, f32[192,768]{1,0:T(8,128)}, /*inde...) custom-call(f32[24,768]{1,0:T(8,128)} %get-tuple-element.24.refs_0_, ...), custom_call_target="tpu_custom_call" | custom-call | tf_op jit(solution)/shard_map/pallas_call | solution.py:510
where the time goes:
time: 150 us; the launch traced here: 149 us
  Pallas kernels  147 us (98%)
    pallas_call x1, Pallas kernels, body(): pl.pallas_call(functools.partial(kernel, nf, nt, limit), out_shape=(small...  137 us
    pallas_call x1, Pallas kernels, body(): pl.pallas_call(settle, grid=(blocks,), out_shape=(small, small, small, sm...  10.9 us

commit v1 on v0

v1 whole, which is shorter than its diff:
```python
import functools

import jax
import jax.numpy as jnp
from jax import lax
from jax.experimental import pallas as pl
from jax.experimental.pallas import tpu as pltpu
from jax.sharding import PartitionSpec as P

MESH = pl.DeviceIdType.MESH
F32 = jnp.float32
BF16 = jnp.bfloat16
UNROLL = 16
TILE = 128


def loop(start, stop, body):
    if stop - start <= UNROLL:
        for i in range(start, stop):
            body(i)
    else:

        @pl.loop(start, stop)
        def _(i):
            body(i)


def mod(value, n):
    return lax.rem(value + 2 * n, n)


def kernel(
    nf,
    nt,
    limit,
    x_hbm,
    y_hbm,
    rec_hbm,
    logit_hbm,
    fcot_hbm,
    lower_ref,
    basis_in_hbm,
    basis_out_hbm,
    m_in,
    s_in,
    m_out,
    s_out,
    w_in,
    w_out,
    mn_in,
    sn_in,
    mn_out,
    sn_out,
    wn_in,
    wn_out,
    copy_in,
    copy_out,
    data,
    logit,
    fcot,
    cots,
    bas,
    own_bas,
    coded,
    term,
    part,
    peer,
    hop,
    step,
    flat,
    small,
    fresh,
    old,
    new,
    cp,
    tots,
    load_sem,
    base_sem,
    out_sem,
    send_a,
    ring_a,
    pair_a,
    send_b,
    ring_b,
    sum_sem,
    swap_sem,
    tot_sem,
    send_d,
    ring_d,
    pair_d,
    send_f,
    ring_f,
    pair_f,
):
    f = lax.axis_index("fs")
    tp = lax.axis_index("tp")
    q = lax.rem(tp, 2)
    n = nf // 2
    z = n // 2
    core = lax.rem(f, 2)
    chip = f // 2
    row, column = chip // 2, lax.rem(chip, 2)
    me = (1 - column) * row + column * (n - 1 - row)
    partner = (f + 1 - 2 * core, tp)
    across = (f, tp + 1 - 2 * q)

    def chip_at(position):
        side = position // z
        return 2 * ((1 - side) * position + side * (n - 1 - position)) + side

    def dev_at(position):
        return chip_at(position) * 2 + core

    depth = basis_in_hbm.shape[0]
    half = depth // 2
    units = cots.shape[2]
    span = part.shape[2]
    lanes = 2 if units % 256 == 0 else 1
    width = units // lanes

    def own(ref, dev):
        return ref.at[pl.ds(pl.multiple_of(dev * depth, depth), depth)]

    def fetch(src, dst, i):
        return pltpu.make_async_copy(src, dst, load_sem.at[i])

    def pick(i, first, second, dst, sem):
        @pl.when(q == 0)
        def _():
            pltpu.make_async_copy(first, dst, sem).start()

        @pl.when(q == 1)
        def _():
            pltpu.make_async_copy(second, dst, sem).start()

        return pltpu.make_async_copy(first, dst, sem)

    own_load = pick(0, basis_in_hbm, basis_out_hbm, own(bas, f), base_sem.at[0])
    gate_loads = [fetch(logit_hbm, logit, 0), fetch(fcot_hbm, fcot, 1)]
    for copy in gate_loads:
        copy.start()
    data_load = pick(1, x_hbm, y_hbm, data, base_sem.at[1])
    late_loads = [
        fetch(src, dst, 2 + i)
        for i, (src, dst) in enumerate(
            (
                (rec_hbm, cots.at[1]),
                (m_in, small.at[0]),
                (s_in, small.at[1]),
                (m_out, small.at[2]),
                (s_out, small.at[3]),
                (basis_in_hbm, own_bas.at[0]),
                (basis_out_hbm, own_bas.at[1]),
                (w_in, old.at[0]),
                (w_out, old.at[1]),
            )
        )
    ]
    for copy in late_loads:
        copy.start()

    barrier = pltpu.get_barrier_semaphore()
    everyone = nf * nt
    my_id = f * nt + tp

    def other(i):
        target = lax.rem(my_id + i, everyone)
        return (target // nt, lax.rem(target, nt))

    @pl.loop(1, everyone)
    def _(i):
        pl.semaphore_signal(barrier, inc=1, device_id=other(i), device_id_type=MESH)

    pl.semaphore_wait(barrier, everyone - 1)

    far = n // 2
    near = n - 1 - far
    two_way = ((0, 1, far), (1, -1, far), (0, -1, near), (1, 1, near))

    def neighbour(way):
        return (dev_at(mod(me + way, n)), tp)

    def send(src, dst, sems, target):
        return pltpu.make_async_remote_copy(
            src_ref=src,
            dst_ref=dst,
            send_sem=sems[0],
            recv_sem=sems[1],
            device_id=target,
            device_id_type=MESH,
        )

    def gather(view, chunks, send_sem, ring_sem, pair_sem, between=None):
        flows = two_way

        def remote(j, s, c, sems, target):
            t, way, _ = flows[j]
            block = view(t, dev_at(mod(me - way * s, n)), c)
            return send(block, block, sems, target)

        def ring_copy(j, s, c):
            sems = send_sem.at[j, s, c], ring_sem.at[j, s, c]
            return remote(j, s, c, sems, neighbour(flows[j][1]))

        def pair_copy(j, s, c):
            sems = pair_sem.at[0, j, s, c], pair_sem.at[1, j, s, c]
            return remote(j, s, c, sems, partner)

        def each(s, act):
            for c in range(chunks):
                for j in range(len(flows)):
                    act(j, s, c)

        def move(j, s, c, first=False, last=False):
            if not first:
                ring_copy(j, s - 1, c).wait_recv()
            if not last:
                ring_copy(j, s, c).start()
            if not first or j < 2:
                pair_copy(j, s, c).start()

        each(0, functools.partial(move, first=True))
        if between is not None:
            between()
        loop(1, near, lambda s: each(s, move))
        for s in range(near, far + 1):
            for c in range(chunks):
                for j, (_, _, hops) in enumerate(flows):
                    if s <= hops:
                        move(j, s, c, last=s == hops)

        def finish(j, s, c):
            pair_copy(j, s, c).wait()

        def sent(j, s, c):
            ring_copy(j, s, c).wait_send()

        for c in range(chunks):
            for j, (_, _, hops) in enumerate(flows):
                if j < 2:
                    finish(j, 0, c)
                for s in range(near, hops):
                    sent(j, s, c)
                for s in range(near, hops + 1):
                    finish(j, s, c)
        loop(1, near, lambda s: each(s, finish))
        loop(0, near, lambda s: each(s, sent))

    def make_gate():
        for copy in gate_loads:
            copy.wait()
        tile = 64

        @pl.loop(0, cots.shape[1] // tile)
        def _(i):
            at = pl.ds(pl.multiple_of(i * tile, tile), tile)
            for k in range(units // TILE):
                to = slice(k * TILE, (k + 1) * TILE)
                sig = jax.nn.sigmoid(logit[at, to].astype(F32))
                cots[0, at, to] = (
                    fcot[at, to].astype(F32)
                    * (1.0 - lower_ref[k : k + 1, :])
                    * sig
                    * (1.0 - sig)
                ).astype(BF16)

    own_load.wait()
    gather(
        lambda t, dev, c: bas.at[
            pl.ds(pl.multiple_of(dev * depth + t * half, half), half)
        ],
        1,
        send_a,
        ring_a,
        pair_a,
        make_gate,
    )
    data_load.wait()

    def piece(i):
        return pl.ds(pl.multiple_of(i * TILE, TILE), TILE)

    def swap(i):
        sems = swap_sem.at[0, i], swap_sem.at[1, i]
        return send(coded.at[0, piece(i)], coded.at[1, piece(i)], sems, across)

    tiles = data.shape[0] // TILE

    @pl.loop(0, tiles)
    def _(i):
        coded[0, piece(i)] = jnp.dot(
            data[piece(i)], bas[...], preferred_element_type=F32
        ).astype(BF16)
        swap(i).start()

    def project(k):
        t = q if k == 0 else 1 - q
        for c in range(lanes):
            at = slice(c * width, (c + 1) * width)
            term[:, at] = lax.dot_general(
                coded[k], cots[t, :, at], (((0,), (0,)), ((), ())), preferred_element_type=F32
            )
        for i in range(nf):
            part[k * 2 + i % 2, i // 2] = term[i * span : (i + 1) * span]

    def pair_sum(k):
        sems = sum_sem.at[0, k], sum_sem.at[1, k]
        return send(part.at[k * 2 + 1 - core], peer.at[k], sems, partner)

    def ring_add(j, s, c):
        at = pl.ds(c * width, width)
        sems = send_b.at[j, s, c], ring_b.at[j, s, c]
        return send(hop.at[j, s, :, at], hop.at[j, s + 1, :, at], sems, neighbour(two_way[j][1]))

    def mine(j, s, c):
        k, way, hops = two_way[j]
        at = pl.ds(c * width, width)
        place = chip_at(mod(me + way * (hops - s), n))
        return part[k * 2 + core, place, :, at] + peer[k, place, :, at]

    def begin(k):
        pair_sum(k).wait_recv()
        for c in range(lanes):
            at = pl.ds(c * width, width)
            for j in (k, k + 2):
                if two_way[j][2] > 0:
                    hop[j, 0, :, at] = mine(j, 0, c)
                    ring_add(j, 0, c).start()

    def relay(j, s, c):
        at = pl.ds(c * width, width)
        ring_add(j, s - 1, c).wait_recv()
        hop[j, s, :, at] = hop[j, s, :, at] + mine(j, s, c)
        ring_add(j, s, c).start()

    def relay_all(k, s):
        for c in range(lanes):
            for j in (k, k + 2):
                if isinstance(s, int) and s >= two_way[j][2]:
                    continue
                relay(j, s, c)

    def settle_sum(k):
        for c in range(lanes):
            at = pl.ds(c * width, width)
            ring_add(k + 2, near - 1, c).wait_recv()
            kept = hop[k + 2, near, :, at] + mine(k + 2, near, c)
            ring_add(k, far - 1, c).wait_recv()
            hop[k, far, :, at] = hop[k, far, :, at] + kept

    late_loads[0].wait()
    project(0)
    pair_sum(0).start()
    begin(0)
    early = max(1, near - 1)
    loop(1, early, lambda s: relay_all(0, s))

    @pl.loop(0, tiles)
    def _(i):
        swap(i).wait_recv()

    project(1)
    pair_sum(1).start()
    for s in range(early, far):
        relay_all(0, s)
    begin(1)
    settle_sum(0)
    loop(1, near, lambda s: relay_all(1, s))
    for s in range(near, far):
        relay_all(1, s)
    settle_sum(1)

    low = [hop[k, far] for k in range(2)]
    square = jnp.sum(low[0] * low[0] + low[1] * low[1], axis=(0, 1), keepdims=True)
    tots[my_id] = jnp.broadcast_to(square, tots.shape[1:])

    def tell(i):
        return send(tots.at[my_id], tots.at[my_id], (tot_sem.at[0], tot_sem.at[1]), other(i))

    @pl.loop(1, everyone)
    def _(i):
        tell(i).start()

    def sent_all(s):
        for c in range(lanes):
            for j in range(4):
                ring_add(j, s, c).wait_send()

    loop(0, near, sent_all)
    for s in range(near, far):
        for c in range(lanes):
            for j in range(2):
                ring_add(j, s, c).wait_send()
    for k in range(2):
        pair_sum(k).wait_send()

    @pl.loop(0, tiles)
    def _(i):
        swap(i).wait_send()

    for copy in late_loads[1:]:
        copy.wait()
    all_tots = tots.at[pl.ds(0, everyone - 1)]
    pltpu.make_async_copy(all_tots, all_tots, tot_sem.at[1]).wait()
    pltpu.make_async_copy(all_tots, all_tots, tot_sem.at[0]).wait()

    total = jnp.sum(tots[...], axis=0)
    clip = jnp.minimum(1.0, jnp.sqrt(F32(limit)) * lax.rsqrt(total + 1e-06))[0:1, 0:1]
    for t in range(2):
        grad = clip * hop[lax.rem(q + t, 2), far]
        moment = 0.8 * small[2 * t] + 0.2 * grad
        second = 0.9 * small[2 * t + 1] + 0.1 * grad * grad
        fresh[2 * t] = moment
        fresh[2 * t + 1] = second
        step[t, f] = moment / (jnp.sqrt(second) + 1e-08)

    puts = [
        pltpu.make_async_copy(fresh.at[i], dst, out_sem.at[i])
        for i, dst in enumerate((mn_in, sn_in, mn_out, sn_out))
    ] + [
        pltpu.make_async_copy(new.at[t], dst, out_sem.at[4 + t])
        for t, dst in enumerate((wn_in, wn_out))
    ]

    gather(
        lambda t, dev, c: step.at[t, dev, :, pl.ds(c * width, width)],
        lanes,
        send_d,
        ring_d,
        pair_d,
    )
    for copy in puts[:4]:
        copy.start()

    cut = send_f.shape[2]
    slab = depth // cut
    ways = (1, -1)

    def block(t, s, c):
        dev = dev_at(mod(me - ways[t] * s, n))
        return cp.at[t, pl.ds(pl.multiple_of(dev * depth + c * slab, slab), slab)]

    def pass_on(t, s, c):
        sems = send_f.at[t, s, c], ring_f.at[t, s, c]
        return send(block(t, s, c), block(t, s, c), sems, neighbour(ways[t]))

    def share(t, s, c):
        sems = pair_f.at[0, t, s, c], pair_f.at[1, t, s, c]
        return send(block(t, s, c), block(t, s, c), sems, partner)

    outs = (copy_in, copy_out)

    def put(t, s):
        place = chip_at(mod(me - ways[t] * s, n))
        rows = pl.ds(pl.multiple_of(place * 2 * depth, 2 * depth), 2 * depth)
        return pltpu.make_async_copy(
            cp.at[t, rows], outs[t].at[rows], out_sem.at[6 + t]
        )

    for t in range(2):
        for k in range(nf):
            flat[k * span : (k + 1) * span] = step[t, k]
        whole = flat[...]
        high = whole.astype(BF16)
        rest = (whole - high.astype(F32)).astype(BF16)
        mat = own_bas[t]
        update = jnp.dot(mat, rest, preferred_element_type=F32) + jnp.dot(
            mat, high, preferred_element_type=F32
        )
        made = old[t] - 0.01 * update
        new[t] = made
        cp[t, pl.ds(pl.multiple_of(f * depth, depth), depth)] = made.astype(BF16)
        for c in range(cut):
            pass_on(t, 0, c).start()
        for c in range(cut):
            share(t, 0, c).start()
    for copy in puts[4:]:
        copy.start()

    def gone(s):
        for t in range(2):
            for c in range(cut):
                share(t, s, c).wait()
            put(t, s).start()

    def forward(s):
        for c in range(cut):
            for t in range(2):
                pass_on(t, s - 1, c).wait_recv()
                pass_on(t, s, c).start()
                share(t, s, c).start()
        gone(s - 1)

    loop(1, n - 1, forward)
    for c in range(cut):
        for t in range(2):
            pass_on(t, n - 2, c).wait_recv()
            share(t, n - 1, c).start()
    gone(n - 2)
    gone(n - 1)

    def left(s):
        for c in range(cut):
            for t in range(2):
                pass_on(t, s, c).wait_send()

    loop(0, n - 1, left)
    for copy in puts:
        copy.wait()
    for t in range(2):
        pltpu.make_async_copy(cp.at[t], outs[t], out_sem.at[6 + t]).wait()


def settle(*refs):
    ins, outs = refs[:8], refs[8:16]
    held, tall, wide, in_sem, out_sem = refs[16:22], refs[22], refs[23], refs[24], refs[25]
    blocks = tall.shape[1]
    size = tall.shape[2]

    def rows(i):
        return pl.ds(i * size, size)

    def get(t, i):
        return pltpu.make_async_copy(ins[6 + t].at[rows(i)], tall.at[t, i], in_sem.at[t, i])

    def put(t, i):
        if t == 0:
            return pltpu.make_async_copy(tall.at[0, i], outs[6].at[rows(i)], out_sem.at[0, i])
        return pltpu.make_async_copy(
            wide.at[:, rows(i)], outs[7].at[:, rows(i)], out_sem.at[1, i]
        )

    more = [
        (
            pltpu.make_async_copy(src, mid, in_sem.at[2, i]),
            pltpu.make_async_copy(mid, dst, out_sem.at[2, i]),
        )
        for i, (src, mid, dst) in enumerate(zip(ins[:6], held, outs[:6]))
    ]
    for i in range(blocks):
        for t in (1, 0):
            get(t, i).start()
    for load, _ in more:
        load.start()
    for i in range(blocks):
        get(1, i).wait()
        wide[:, rows(i)] = tall[1, i].T
        put(1, i).start()
        get(0, i).wait()
        put(0, i).start()
    for load, save in more:
        load.wait()
        save.start()
    for i in range(blocks):
        for t in (1, 0):
            put(t, i).wait()
    for _, save in more:
        save.wait()


def body(
    saved_input,
    output_cotangent,
    recurrent_output,
    forget_logit,
    forget_cotangent,
    lower_bound,
    basis_in,
    basis_out,
    moment_in,
    second_in,
    moment_out,
    second_out,
    weight_in,
    weight_out,
):
    nf, nt = lax.axis_size("fs"), lax.axis_size("tp")
    n = nf // 2
    tokens, model = saved_input.shape
    units = recurrent_output.shape[1]
    depth, rank = basis_in.shape
    span = moment_in.shape[0]
    limit = 2.0 * rank * units * nt
    small = jax.ShapeDtypeStruct((span, units), F32)
    weight = jax.ShapeDtypeStruct((depth, units), F32)
    copied = jax.ShapeDtypeStruct((model, units), BF16)
    cut = 2 if depth % 32 == 0 else 1
    lanes = 2 if units % 256 == 0 else 1
    far = n // 2
    hbm = pl.BlockSpec(memory_space=pl.ANY)
    vmem = pl.BlockSpec(memory_space=pltpu.VMEM)
    dma = pltpu.SemaphoreType.DMA
    outs = pl.pallas_call(
        functools.partial(kernel, nf, nt, limit),
        out_shape=(small, small, small, small, weight, weight, copied, copied),
        in_specs=[hbm] * 5 + [vmem] + [hbm] * 8,
        out_specs=[hbm] * 8,
        scratch_shapes=[
            pltpu.VMEM((tokens, model), BF16),
            pltpu.VMEM((tokens, units), BF16),
            pltpu.VMEM((tokens, units), BF16),
            pltpu.VMEM((2, tokens, units), BF16),
            pltpu.VMEM((model, rank), BF16),
            pltpu.VMEM((2, depth, rank), BF16),
            pltpu.VMEM((2, tokens, rank), BF16),
            pltpu.VMEM((rank, units), F32),
            pltpu.VMEM((4, n, span, units), F32),
            pltpu.VMEM((2, n, span, units), F32),
            pltpu.VMEM((4, far + 1, span, units), F32),
            pltpu.VMEM((2, nf, span, units), F32),
            pltpu.VMEM((rank, units), F32),
            pltpu.VMEM((4, span, units), F32),
            pltpu.VMEM((4, span, units), F32),
            pltpu.VMEM((2, depth, units), F32),
            pltpu.VMEM((2, depth, units), F32),
            pltpu.VMEM((2, model, units), BF16),
            pltpu.VMEM((nf * nt, 8, 128), F32),
            dma((11,)),
            dma((2,)),
            dma((8,)),
            dma((4, far, 1)),
            dma((4, far, 1)),
            dma((2, 4, far + 1, 1)),
            dma((4, far, lanes)),
            dma((4, far, lanes)),
            dma((2, 2)),
            dma((2, tokens // TILE)),
            dma((2,)),
            dma((4, far, lanes)),
            dma((4, far, lanes)),
            dma((2, 4, far + 1, lanes)),
            dma((2, n - 1, cut)),
            dma((2, n - 1, cut)),
            dma((2, 2, n, cut)),
        ],
        compiler_params=pltpu.CompilerParams(
            collective_id=0, has_side_effects=True, vmem_limit_bytes=60 * 1024 * 1024
        ),
    )(
        saved_input,
        output_cotangent,
        recurrent_output,
        forget_logit,
        forget_cotangent,
        lower_bound.reshape(units // TILE, TILE),
        basis_in,
        basis_out,
        moment_in,
        second_in,
        moment_out,
        second_out,
        weight_in,
        weight_out.T,
    )
    blocks = 8 if model % 1024 == 0 else 1
    size = model // blocks
    outs = pl.pallas_call(
        settle,
        out_shape=(small, small, small, small, weight, weight, copied)
        + (jax.ShapeDtypeStruct((units, model), BF16),),
        in_specs=[hbm] * 8,
        out_specs=[hbm] * 8,
        scratch_shapes=[pltpu.VMEM((span, units), F32)] * 4
        + [pltpu.VMEM((depth, units), F32)] * 2
        + [
            pltpu.VMEM((2, blocks, size, units), BF16),
            pltpu.VMEM((units, model), BF16),
            dma((3, max(blocks, 6))),
            dma((3, max(blocks, 6))),
        ],
    )(*outs)
    return tuple(outs[:5]) + (outs[5].T, outs[6], outs[7])


def solution(mesh):
    return jax.shard_map(
        body,
        mesh=mesh,
        in_specs=(
            P("fs", None),
            P("fs", None),
            P("fs", "tp"),
            P("fs", "tp"),
            P("fs", "tp"),
            P("tp"),
            P("fs", None),
            P("fs", None),
            P("fs", "tp"),
            P("fs", "tp"),
            P("fs", "tp"),
            P("fs", "tp"),
            P("fs", "tp"),
            P("tp", "fs"),
        ),
        out_specs=(
            P("fs", "tp"),
            P("fs", "tp"),
            P("fs", "tp"),
            P("fs", "tp"),
            P("fs", "tp"),
            P("tp", "fs"),
            P(None, "tp"),
            P("tp", None),
        ),
        check_vma=False,
    )
```

time: 150 us -> 136 us (0.907)
  Pallas kernels: 147 us -> 135 us
    pallas_call x1, Pallas kernels: 137 us -> 127 us  [body(): pl.pallas_call(functools.partial(kernel, nf, nt, limit), out_shape=(small...]
    pallas_call x1, Pallas kernels: 10.9 us -> 8.36 us  [body(): pl.pallas_call(settle, out_shape=(small, small, small, small, weight, wei...]
where the time goes in v1:
time: 136 us
  Pallas kernels  135 us (99%)
    pallas_call x1, Pallas kernels, body(): pl.pallas_call(functools.partial(kernel, nf, nt, limit), out_shape=(small...  127 us
    pallas_call x1, Pallas kernels, body(): pl.pallas_call(settle, out_shape=(small, small, small, small, weight, wei...  8.36 us

profile of v1, /device:TPU:0, one launch (start us, length us, event | category | flops | bytes accessed | tf_op | source)
XLA Modules:
  0.0 135.8 jit_solution(10865993484027234260)
XLA Ops:
  0.6 126.8 %shard_map.197 = (f32[24,768]{1,0:T(8,128)}, f32[24,768]{1,0:T(8,128)}, f32[24,768]{1,0:T(8,128)}, f32[24,768]{1,0:T(8,128)}, f32[192,768]{1,0:T(8,128)}, /*inde...) custom-call(bf16[512,3072]{1,0:T(8,128)(2,1)} %x_hbm.1, bf16[512,3072]{1,0:T(8,128)(2,1)} %y_hbm.1, ...), custom_call_target="tpu_custom_call" | custom-call | tf_op jit(solution)/shard_map/pallas_call | solution.py:593
  127.4 8.4 %shard_map.198 = (f32[24,768]{1,0:T(8,128)}, f32[24,768]{1,0:T(8,128)}, f32[24,768]{1,0:T(8,128)}, f32[24,768]{1,0:T(8,128)}, f32[192,768]{1,0:T(8,128)}, /*inde...) custom-call(f32[24,768]{1,0:T(8,128)} %get-tuple-element.24.refs_0_, ...), custom_call_target="tpu_custom_call" | custom-call | tf_op jit(solution)/shard_map/pallas_call | solution.py:657

commit v2 on v1

--- a/solution.py
+++ b/solution.py
@@ -33,6 +33,7 @@
     nf,
     nt,
     limit,
+    ahead,
     x_hbm,
     y_hbm,
     rec_hbm,
@@ -68,29 +69,32 @@
     hop,
     step,
     flat,
+    split,
     small,
     fresh,
     old,
     new,
     cp,
     tots,
+    pre,
+    lhs,
     load_sem,
     base_sem,
     out_sem,
-    send_a,
+    sem_a,
     ring_a,
-    pair_a,
-    send_b,
+    sem_b,
     ring_b,
     sum_sem,
     swap_sem,
     tot_sem,
-    send_d,
+    sem_d,
     ring_d,
-    pair_d,
-    send_f,
+    sem_f,
     ring_f,
     pair_f,
+    sem_e,
+    ring_e,
 ):
     f = lax.axis_index("fs")
     tp = lax.axis_index("tp")
@@ -190,21 +194,23 @@
             device_id_type=MESH,
         )
 
-    def gather(view, chunks, send_sem, ring_sem, pair_sem, between=None):
+    def arrive(ref, sem):
+        pltpu.make_async_copy(ref, ref, sem).wait()
+
+    def gather(view, chunks, sems, ring_sem, blocks, between=None):
         flows = two_way
 
-        def remote(j, s, c, sems, target):
+        def remote(j, s, c, pair, target):
             t, way, _ = flows[j]
             block = view(t, dev_at(mod(me - way * s, n)), c)
-            return send(block, block, sems, target)
+            return send(block, block, pair, target)
 
         def ring_copy(j, s, c):
-            sems = send_sem.at[j, s, c], ring_sem.at[j, s, c]
-            return remote(j, s, c, sems, neighbour(flows[j][1]))
+            pair = sems.at[0], ring_sem.at[j, s, c]
+            return remote(j, s, c, pair, neighbour(flows[j][1]))
 
         def pair_copy(j, s, c):
-            sems = pair_sem.at[0, j, s, c], pair_sem.at[1, j, s, c]
-            return remote(j, s, c, sems, partner)
+            return remote(j, s, c, (sems.at[1], sems.at[2]), partner)
 
         def each(s, act):
             for c in range(chunks):
@@ -228,23 +234,13 @@
                 for j, (_, _, hops) in enumerate(flows):
                     if s <= hops:
                         move(j, s, c, last=s == hops)
-
-        def finish(j, s, c):
-            pair_copy(j, s, c).wait()
-
-        def sent(j, s, c):
-            ring_copy(j, s, c).wait_send()
-
-        for c in range(chunks):
-            for j, (_, _, hops) in enumerate(flows):
-                if j < 2:
-                    finish(j, 0, c)
-                for s in range(near, hops):
-                    sent(j, s, c)
-                for s in range(near, hops + 1):
-                    finish(j, s, c)
-        loop(1, near, lambda s: each(s, finish))
-        loop(0, near, lambda s: each(s, sent))
+        arrive(blocks(n), sems.at[2])
+
+        def finish():
+            arrive(blocks(n), sems.at[1])
+            arrive(blocks(n - 1), sems.at[0])
+
+        return finish
 
     def make_gate():
         for copy in gate_loads:
@@ -264,24 +260,52 @@
                     * (1.0 - sig)
                 ).astype(BF16)
 
+    ways = (1, -1)
+
+    def ahead_copy(t, s):
+        block = pre.at[t, chip_at(mod(me - ways[t] * s, n))]
+        return send(block, block, (sem_e.at[0], ring_e.at[t, s]), neighbour(ways[t]))
+
+    at_hop = [0]
+
+    def advance():
+        s = at_hop[0]
+        if not ahead or s >= n:
+            return
+        for t in range(2):
+            if s > 0:
+                ahead_copy(t, s - 1).wait_recv()
+            if s < n - 1:
+                ahead_copy(t, s).start()
+        at_hop[0] = s + 1
+
+    def prepare():
+        make_gate()
+        for copy in late_loads[7:]:
+            copy.wait()
+        if ahead:
+            for t in range(2):
+                pre[t, chip] = old[t, :ahead].astype(BF16)
+
     own_load.wait()
-    gather(
+    done_a = gather(
         lambda t, dev, c: bas.at[
             pl.ds(pl.multiple_of(dev * depth + t * half, half), half)
         ],
         1,
-        send_a,
+        sem_a,
         ring_a,
-        pair_a,
-        make_gate,
+        lambda m: bas.at[pl.ds(0, m * depth)],
+        prepare,
     )
+    advance()
     data_load.wait()
 
     def piece(i):
         return pl.ds(pl.multiple_of(i * TILE, TILE), TILE)
 
     def swap(i):
-        sems = swap_sem.at[0, i], swap_sem.at[1, i]
+        sems = swap_sem.at[0], swap_sem.at[1]
         return send(coded.at[0, piece(i)], coded.at[1, piece(i)], sems, across)
 
     tiles = data.shape[0] // TILE
@@ -292,6 +316,19 @@
             data[piece(i)], bas[...], preferred_element_type=F32
         ).astype(BF16)
         swap(i).start()
+
+    def lend(p):
+        at = pl.multiple_of((2 * p + core) * depth, depth)
+        return send(
+            bas.at[pl.ds(at, ahead)],
+            lhs.at[1, pl.ds(p * ahead, ahead)],
+            (sem_e.at[1], sem_e.at[2]),
+            across,
+        )
+
+    if ahead:
+        for p in range(n):
+            lend(p).start()
 
     def project(k):
         t = q if k == 0 else 1 - q
@@ -309,7 +346,7 @@
 
     def ring_add(j, s, c):
         at = pl.ds(c * width, width)
-        sems = send_b.at[j, s, c], ring_b.at[j, s, c]
+        sems = sem_b.at[0], ring_b.at[j, s, c]
         return send(hop.at[j, s, :, at], hop.at[j, s + 1, :, at], sems, neighbour(two_way[j][1]))
 
     def mine(j, s, c):
@@ -352,22 +389,25 @@
     project(0)
     pair_sum(0).start()
     begin(0)
+    advance()
+
+    def relay_on(k, s):
+        relay_all(k, s)
+        advance()
+
     early = max(1, near - 1)
-    loop(1, early, lambda s: relay_all(0, s))
-
-    @pl.loop(0, tiles)
-    def _(i):
-        swap(i).wait_recv()
-
+    loop(1, early, lambda s: relay_on(0, s))
+    arrive(coded.at[1], swap_sem.at[1])
     project(1)
     pair_sum(1).start()
+    advance()
     for s in range(early, far):
-        relay_all(0, s)
+        relay_on(0, s)
     begin(1)
     settle_sum(0)
-    loop(1, near, lambda s: relay_all(1, s))
+    loop(1, near, lambda s: relay_on(1, s))
     for s in range(near, far):
-        relay_all(1, s)
+        relay_on(1, s)
     settle_sum(1)
 
     low = [hop[k, far] for k in range(2)]
@@ -381,28 +421,22 @@
     def _(i):
         tell(i).start()
 
-    def sent_all(s):
-        for c in range(lanes):
-            for j in range(4):
-                ring_add(j, s, c).wait_send()
-
-    loop(0, near, sent_all)
-    for s in range(near, far):
-        for c in range(lanes):
-            for j in range(2):
-                ring_add(j, s, c).wait_send()
+    done_a()
+    arrive(step.at[:, pl.ds(0, n - 1)], sem_b.at[0])
     for k in range(2):
         pair_sum(k).wait_send()
-
-    @pl.loop(0, tiles)
-    def _(i):
-        swap(i).wait_send()
-
-    for copy in late_loads[1:]:
+    arrive(coded.at[0], swap_sem.at[0])
+    for copy in late_loads[1:7]:
         copy.wait()
+    if ahead:
+        arrive(lhs.at[1], sem_e.at[1])
+        arrive(lhs.at[1], sem_e.at[2])
+        for p in range(n):
+            at = pl.multiple_of((2 * p + core) * depth, depth)
+            lhs[0, p * ahead : (p + 1) * ahead] = bas[pl.ds(at, ahead)]
     all_tots = tots.at[pl.ds(0, everyone - 1)]
-    pltpu.make_async_copy(all_tots, all_tots, tot_sem.at[1]).wait()
-    pltpu.make_async_copy(all_tots, all_tots, tot_sem.at[0]).wait()
+    arrive(all_tots, tot_sem.at[1])
+    arrive(all_tots, tot_sem.at[0])
 
     total = jnp.sum(tots[...], axis=0)
     clip = jnp.minimum(1.0, jnp.sqrt(F32(limit)) * lax.rsqrt(total + 1e-06))[0:1, 0:1]
@@ -422,30 +456,30 @@
         for t, dst in enumerate((wn_in, wn_out))
     ]
 
-    gather(
+    for copy in puts[:4]:
+        copy.start()
+    done_d = gather(
         lambda t, dev, c: step.at[t, dev, :, pl.ds(c * width, width)],
         lanes,
-        send_d,
+        sem_d,
         ring_d,
-        pair_d,
+        lambda m: step.at[:, pl.ds(0, m)],
     )
-    for copy in puts[:4]:
-        copy.start()
-
-    cut = send_f.shape[2]
-    slab = depth // cut
-    ways = (1, -1)
+
+    cut = ring_f.shape[2]
+    late = depth - ahead
+    slab = late // cut
 
     def block(t, s, c):
         dev = dev_at(mod(me - ways[t] * s, n))
-        return cp.at[t, pl.ds(pl.multiple_of(dev * depth + c * slab, slab), slab)]
+        return cp.at[t, pl.ds(pl.multiple_of(dev * depth + ahead + c * slab, 16), slab)]
 
     def pass_on(t, s, c):
-        sems = send_f.at[t, s, c], ring_f.at[t, s, c]
+        sems = sem_f.at[0], ring_f.at[t, s, c]
         return send(block(t, s, c), block(t, s, c), sems, neighbour(ways[t]))
 
     def share(t, s, c):
-        sems = pair_f.at[0, t, s, c], pair_f.at[1, t, s, c]
+        sems = sem_f.at[1], pair_f.at[t, s]
         return send(block(t, s, c), block(t, s, c), sems, partner)
 
     outs = (copy_in, copy_out)
@@ -457,19 +491,23 @@
             cp.at[t, rows], outs[t].at[rows], out_sem.at[6 + t]
         )
 
+    rank = flat.shape[0]
+
+    def apply(mat, steps):
+        return jnp.dot(
+            jnp.concatenate([mat, mat], axis=1), steps, preferred_element_type=F32
+        )
+
     for t in range(2):
         for k in range(nf):
             flat[k * span : (k + 1) * span] = step[t, k]
         whole = flat[...]
         high = whole.astype(BF16)
-        rest = (whole - high.astype(F32)).astype(BF16)
-        mat = own_bas[t]
-        update = jnp.dot(mat, rest, preferred_element_type=F32) + jnp.dot(
-            mat, high, preferred_element_type=F32
-        )
-        made = old[t] - 0.01 * update
+        split[t, :rank] = high
+        split[t, rank:] = (whole - high.astype(F32)).astype(BF16)
+        made = old[t] - 0.01 * apply(own_bas[t], split[t])
         new[t] = made
-        cp[t, pl.ds(pl.multiple_of(f * depth, depth), depth)] = made.astype(BF16)
+        cp[t, pl.ds(pl.multiple_of(f * depth + ahead, 16), late)] = made[ahead:].astype(BF16)
         for c in range(cut):
             pass_on(t, 0, c).start()
         for c in range(cut):
@@ -477,10 +515,36 @@
     for copy in puts[4:]:
         copy.start()
 
+    def rows_of(t, p):
+        at = pl.multiple_of((2 * p + core) * depth, depth)
+        return cp.at[t, pl.ds(at, ahead)]
+
+    if ahead:
+        while at_hop[0] < n:
+            advance()
+        group = max(1, 256 // ahead)
+        for k in range(2):
+            t = q if k == 0 else 1 - q
+            for p in range(0, n, group):
+                size = min(group, n - p)
+                moved = apply(lhs[k, p * ahead : (p + size) * ahead], split[t])
+                for i in range(size):
+                    kept = pre[t, p + i].astype(F32)
+                    rows_of(t, p + i)[...] = (
+                        kept - 0.01 * moved[i * ahead : (i + 1) * ahead]
+                    ).astype(BF16)
+                    send(
+                        rows_of(t, p + i),
+                        rows_of(t, p + i),
+                        (sem_e.at[3], sem_e.at[4]),
+                        partner,
+                    ).start()
+        arrive(pre, sem_e.at[4])
+
     def gone(s):
         for t in range(2):
-            for c in range(cut):
-                share(t, s, c).wait()
+            whole_block = cp.at[t, pl.ds(0, late)]
+            arrive(whole_block, pair_f.at[t, s])
             put(t, s).start()
 
     def forward(s):
@@ -499,12 +563,12 @@
     gone(n - 2)
     gone(n - 1)
 
-    def left(s):
-        for c in range(cut):
-            for t in range(2):
-                pass_on(t, s, c).wait_send()
-
-    loop(0, n - 1, left)
+    arrive(cp.at[:, pl.ds(0, (n - 1) * late)], sem_f.at[0])
+    arrive(cp.at[:, pl.ds(0, n * late)], sem_f.at[1])
+    if ahead:
+        arrive(pre, sem_e.at[3])
+        arrive(pre.at[:, pl.ds(0, n - 1)], sem_e.at[0])
+    done_d()
     for copy in puts:
         copy.wait()
     for t in range(2):
@@ -587,11 +651,12 @@
     cut = 2 if depth % 32 == 0 else 1
     lanes = 2 if units % 256 == 0 else 1
     far = n // 2
+    ahead = depth // 3 // 16 * 16
     hbm = pl.BlockSpec(memory_space=pl.ANY)
     vmem = pl.BlockSpec(memory_space=pltpu.VMEM)
     dma = pltpu.SemaphoreType.DMA
     outs = pl.pallas_call(
-        functools.partial(kernel, nf, nt, limit),
+        functools.partial(kernel, nf, nt, limit, ahead),
         out_shape=(small, small, small, small, weight, weight, copied, copied),
         in_specs=[hbm] * 5 + [vmem] + [hbm] * 8,
         out_specs=[hbm] * 8,
@@ -609,29 +674,32 @@
             pltpu.VMEM((4, far + 1, span, units), F32),
             pltpu.VMEM((2, nf, span, units), F32),
             pltpu.VMEM((rank, units), F32),
+            pltpu.VMEM((2, 2 * rank, units), BF16),
             pltpu.VMEM((4, span, units), F32),
             pltpu.VMEM((4, span, units), F32),
             pltpu.VMEM((2, depth, units), F32),
             pltpu.VMEM((2, depth, units), F32),
             pltpu.VMEM((2, model, units), BF16),
             pltpu.VMEM((nf * nt, 8, 128), F32),
+            pltpu.VMEM((2, n, max(ahead, 16), units), BF16),
+            pltpu.VMEM((2, n * max(ahead, 16), rank), BF16),
             dma((11,)),
             dma((2,)),
             dma((8,)),
+            dma((3,)),
             dma((4, far, 1)),
-            dma((4, far, 1)),
-            dma((2, 4, far + 1, 1)),
-            dma((4, far, lanes)),
+            dma((1,)),
             dma((4, far, lanes)),
             dma((2, 2)),
-            dma((2, tokens // TILE)),
             dma((2,)),
+            dma((2,)),
+            dma((3,)),
             dma((4, far, lanes)),
-            dma((4, far, lanes)),
-            dma((2, 4, far + 1, lanes)),
+            dma((2,)),
             dma((2, n - 1, cut)),
-            dma((2, n - 1, cut)),
-            dma((2, 2, n, cut)),
+            dma((2, n)),
+            dma((5,)),
+            dma((2, n - 1)),
         ],
         compiler_params=pltpu.CompilerParams(
             collective_id=0, has_side_effects=True, vmem_limit_bytes=60 * 1024 * 1024

time: 136 us -> 131 us (0.963)
  Pallas kernels: 135 us -> 130 us
    pallas_call x1, Pallas kernels: 127 us -> 122 us  [body(): pl.pallas_call(functools.partial(kernel, nf, nt, limit, ahead), out_shape...]
where the time goes in v2:
time: 131 us
  Pallas kernels  130 us (99%)
    pallas_call x1, Pallas kernels, body(): pl.pallas_call(functools.partial(kernel, nf, nt, limit, ahead), out_shape...  122 us
    pallas_call x1, Pallas kernels, body(): pl.pallas_call(settle, out_shape=(small, small, small, small, weight, wei...  8.36 us

profile of v2, /device:TPU:0, one launch (start us, length us, event | category | flops | bytes accessed | tf_op | source)
XLA Modules:
  0.0 130.7 jit_solution(883767563337835883)
XLA Ops:
  0.6 121.7 %shard_map.197 = (f32[24,768]{1,0:T(8,128)}, f32[24,768]{1,0:T(8,128)}, f32[24,768]{1,0:T(8,128)}, f32[24,768]{1,0:T(8,128)}, f32[192,768]{1,0:T(8,128)}, /*inde...) custom-call(bf16[512,3072]{1,0:T(8,128)(2,1)} %x_hbm.1, bf16[512,3072]{1,0:T(8,128)(2,1)} %y_hbm.1, ...), custom_call_target="tpu_custom_call" | custom-call | tf_op jit(solution)/shard_map/pallas_call | solution.py:658
  122.3 8.4 %shard_map.198 = (f32[24,768]{1,0:T(8,128)}, f32[24,768]{1,0:T(8,128)}, f32[24,768]{1,0:T(8,128)}, f32[24,768]{1,0:T(8,128)}, f32[192,768]{1,0:T(8,128)}, /*inde...) custom-call(f32[24,768]{1,0:T(8,128)} %get-tuple-element.24.refs_0_, ...), custom_call_target="tpu_custom_call" | custom-call | tf_op jit(solution)/shard_map/pallas_call | solution.py:725

commit v3 on v2

--- a/solution.py
+++ b/solution.py
@@ -48,14 +48,9 @@
     s_out,
     w_in,
     w_out,
-    mn_in,
-    sn_in,
-    mn_out,
-    sn_out,
-    wn_in,
-    wn_out,
-    copy_in,
-    copy_out,
+    fresh,
+    new,
+    cp,
     data,
     logit,
     fcot,
@@ -71,16 +66,12 @@
     flat,
     split,
     small,
-    fresh,
     old,
-    new,
-    cp,
     tots,
     pre,
     lhs,
     load_sem,
     base_sem,
-    out_sem,
     sem_a,
     ring_a,
     sem_b,
@@ -197,7 +188,7 @@
     def arrive(ref, sem):
         pltpu.make_async_copy(ref, ref, sem).wait()
 
-    def gather(view, chunks, sems, ring_sem, blocks, between=None):
+    def gather(view, chunks, sems, ring_sem, blocks, between=None, after=None):
         flows = two_way
 
         def remote(j, s, c, pair, target):
@@ -234,6 +225,8 @@
                 for j, (_, _, hops) in enumerate(flows):
                     if s <= hops:
                         move(j, s, c, last=s == hops)
+        if after is not None:
+            after()
         arrive(blocks(n), sems.at[2])
 
         def finish():
@@ -297,8 +290,8 @@
         ring_a,
         lambda m: bas.at[pl.ds(0, m * depth)],
         prepare,
+        advance,
     )
-    advance()
     data_load.wait()
 
     def piece(i):
@@ -388,26 +381,24 @@
     late_loads[0].wait()
     project(0)
     pair_sum(0).start()
+    advance()
     begin(0)
+    early = max(1, near - 1)
+    loop(1, early, lambda s: relay_all(0, s))
     advance()
-
-    def relay_on(k, s):
-        relay_all(k, s)
-        advance()
-
-    early = max(1, near - 1)
-    loop(1, early, lambda s: relay_on(0, s))
     arrive(coded.at[1], swap_sem.at[1])
     project(1)
     pair_sum(1).start()
+    loop(early, near, lambda s: relay_all(0, s))
+    begin(1)
     advance()
-    for s in range(early, far):
-        relay_on(0, s)
-    begin(1)
+    for s in range(near, far):
+        relay_all(0, s)
+    loop(1, near, lambda s: relay_all(1, s))
+    advance()
     settle_sum(0)
-    loop(1, near, lambda s: relay_on(1, s))
     for s in range(near, far):
-        relay_on(1, s)
+        relay_all(1, s)
     settle_sum(1)
 
     low = [hop[k, far] for k in range(2)]
@@ -420,6 +411,8 @@
     @pl.loop(1, everyone)
     def _(i):
         tell(i).start()
+
+    advance()
 
     done_a()
     arrive(step.at[:, pl.ds(0, n - 1)], sem_b.at[0])
@@ -448,22 +441,14 @@
         fresh[2 * t + 1] = second
         step[t, f] = moment / (jnp.sqrt(second) + 1e-08)
 
-    puts = [
-        pltpu.make_async_copy(fresh.at[i], dst, out_sem.at[i])
-        for i, dst in enumerate((mn_in, sn_in, mn_out, sn_out))
-    ] + [
-        pltpu.make_async_copy(new.at[t], dst, out_sem.at[4 + t])
-        for t, dst in enumerate((wn_in, wn_out))
-    ]
-
-    for copy in puts[:4]:
-        copy.start()
     done_d = gather(
         lambda t, dev, c: step.at[t, dev, :, pl.ds(c * width, width)],
         lanes,
         sem_d,
         ring_d,
         lambda m: step.at[:, pl.ds(0, m)],
+        None,
+        advance,
     )
 
     cut = ring_f.shape[2]
@@ -481,15 +466,6 @@
     def share(t, s, c):
         sems = sem_f.at[1], pair_f.at[t, s]
         return send(block(t, s, c), block(t, s, c), sems, partner)
-
-    outs = (copy_in, copy_out)
-
-    def put(t, s):
-        place = chip_at(mod(me - ways[t] * s, n))
-        rows = pl.ds(pl.multiple_of(place * 2 * depth, 2 * depth), 2 * depth)
-        return pltpu.make_async_copy(
-            cp.at[t, rows], outs[t].at[rows], out_sem.at[6 + t]
-        )
 
     rank = flat.shape[0]
 
@@ -512,9 +488,6 @@
             pass_on(t, 0, c).start()
         for c in range(cut):
             share(t, 0, c).start()
-    for copy in puts[4:]:
-        copy.start()
-
     def rows_of(t, p):
         at = pl.multiple_of((2 * p + core) * depth, depth)
         return cp.at[t, pl.ds(at, ahead)]
@@ -545,7 +518,6 @@
         for t in range(2):
             whole_block = cp.at[t, pl.ds(0, late)]
             arrive(whole_block, pair_f.at[t, s])
-            put(t, s).start()
 
     def forward(s):
         for c in range(cut):
@@ -569,56 +541,31 @@
         arrive(pre, sem_e.at[3])
         arrive(pre.at[:, pl.ds(0, n - 1)], sem_e.at[0])
     done_d()
-    for copy in puts:
-        copy.wait()
-    for t in range(2):
-        pltpu.make_async_copy(cp.at[t], outs[t], out_sem.at[6 + t]).wait()
-
-
-def settle(*refs):
-    ins, outs = refs[:8], refs[8:16]
-    held, tall, wide, in_sem, out_sem = refs[16:22], refs[22], refs[23], refs[24], refs[25]
-    blocks = tall.shape[1]
-    size = tall.shape[2]
-
-    def rows(i):
-        return pl.ds(i * size, size)
-
-    def get(t, i):
-        return pltpu.make_async_copy(ins[6 + t].at[rows(i)], tall.at[t, i], in_sem.at[t, i])
-
-    def put(t, i):
-        if t == 0:
-            return pltpu.make_async_copy(tall.at[0, i], outs[6].at[rows(i)], out_sem.at[0, i])
-        return pltpu.make_async_copy(
-            wide.at[:, rows(i)], outs[7].at[:, rows(i)], out_sem.at[1, i]
+
+
+def settle(fresh, new, cp, *refs):
+    outs, wide, sem = refs[:8], refs[8], refs[9]
+    model = cp.shape[1]
+    size = sem.shape[0]
+    blocks = size - 8
+    step = model // blocks
+    saves = [
+        pltpu.make_async_copy(src, dst, sem.at[blocks + i])
+        for i, (src, dst) in enumerate(
+            [(fresh.at[i], outs[i]) for i in range(4)]
+            + [(new.at[i], outs[4 + i]) for i in range(2)]
+            + [(cp.at[0], outs[6])]
         )
-
-    more = [
-        (
-            pltpu.make_async_copy(src, mid, in_sem.at[2, i]),
-            pltpu.make_async_copy(mid, dst, out_sem.at[2, i]),
-        )
-        for i, (src, mid, dst) in enumerate(zip(ins[:6], held, outs[:6]))
     ]
-    for i in range(blocks):
-        for t in (1, 0):
-            get(t, i).start()
-    for load, _ in more:
-        load.start()
-    for i in range(blocks):
-        get(1, i).wait()
-        wide[:, rows(i)] = tall[1, i].T
-        put(1, i).start()
-        get(0, i).wait()
-        put(0, i).start()
-    for load, save in more:
-        load.wait()
+    saves = saves[::-1]
+    for save in saves:
         save.start()
     for i in range(blocks):
-        for t in (1, 0):
-            put(t, i).wait()
-    for _, save in more:
+        at = pl.ds(i * step, step)
+        wide[:, at] = cp[1, at].T
+        saves.append(pltpu.make_async_copy(wide.at[:, at], outs[7].at[:, at], sem.at[i]))
+        saves[-1].start()
+    for save in saves:
         save.wait()
 
 
@@ -648,18 +595,23 @@
     small = jax.ShapeDtypeStruct((span, units), F32)
     weight = jax.ShapeDtypeStruct((depth, units), F32)
     copied = jax.ShapeDtypeStruct((model, units), BF16)
+    held = (
+        jax.ShapeDtypeStruct((4, span, units), F32),
+        jax.ShapeDtypeStruct((2, depth, units), F32),
+        jax.ShapeDtypeStruct((2, model, units), BF16),
+    )
     cut = 2 if depth % 32 == 0 else 1
     lanes = 2 if units % 256 == 0 else 1
     far = n // 2
     ahead = depth // 3 // 16 * 16
-    hbm = pl.BlockSpec(memory_space=pl.ANY)
+    hbm = pl.BlockSpec(memory_space=pltpu.HBM)
     vmem = pl.BlockSpec(memory_space=pltpu.VMEM)
     dma = pltpu.SemaphoreType.DMA
     outs = pl.pallas_call(
         functools.partial(kernel, nf, nt, limit, ahead),
-        out_shape=(small, small, small, small, weight, weight, copied, copied),
+        out_shape=tuple(pltpu.VMEM(o.shape, o.dtype) for o in held),
         in_specs=[hbm] * 5 + [vmem] + [hbm] * 8,
-        out_specs=[hbm] * 8,
+        out_specs=[vmem] * 3,
         scratch_shapes=[
             pltpu.VMEM((tokens, model), BF16),
             pltpu.VMEM((tokens, units), BF16),
@@ -676,16 +628,12 @@
             pltpu.VMEM((rank, units), F32),
             pltpu.VMEM((2, 2 * rank, units), BF16),
             pltpu.VMEM((4, span, units), F32),
-            pltpu.VMEM((4, span, units), F32),
             pltpu.VMEM((2, depth, units), F32),
-            pltpu.VMEM((2, depth, units), F32),
-            pltpu.VMEM((2, model, units), BF16),
             pltpu.VMEM((nf * nt, 8, 128), F32),
             pltpu.VMEM((2, n, max(ahead, 16), units), BF16),
             pltpu.VMEM((2, n * max(ahead, 16), rank), BF16),
             dma((11,)),
             dma((2,)),
-            dma((8,)),
             dma((3,)),
             dma((4, far, 1)),
             dma((1,)),
@@ -702,7 +650,7 @@
             dma((2, n - 1)),
         ],
         compiler_params=pltpu.CompilerParams(
-            collective_id=0, has_side_effects=True, vmem_limit_bytes=60 * 1024 * 1024
+            collective_id=0, has_side_effects=True, vmem_limit_bytes=50 * 1024 * 1024
         ),
     )(
         saved_input,
@@ -721,21 +669,14 @@
         weight_out.T,
     )
     blocks = 8 if model % 1024 == 0 else 1
-    size = model // blocks
     outs = pl.pallas_call(
         settle,
         out_shape=(small, small, small, small, weight, weight, copied)
         + (jax.ShapeDtypeStruct((units, model), BF16),),
-        in_specs=[hbm] * 8,
+        in_specs=[vmem] * 3,
         out_specs=[hbm] * 8,
-        scratch_shapes=[pltpu.VMEM((span, units), F32)] * 4
-        + [pltpu.VMEM((depth, units), F32)] * 2
-        + [
-            pltpu.VMEM((2, blocks, size, units), BF16),
-            pltpu.VMEM((units, model), BF16),
-            dma((3, max(blocks, 6))),
-            dma((3, max(blocks, 6))),
-        ],
+        scratch_shapes=[pltpu.VMEM((units, model), BF16), dma((blocks + 8,))],
+        compiler_params=pltpu.CompilerParams(vmem_limit_bytes=40 * 1024 * 1024),
     )(*outs)
     return tuple(outs[:5]) + (outs[5].T, outs[6], outs[7])
 

time: 131 us -> 115 us (0.88)
  Pallas kernels: 130 us -> 114 us
    pallas_call x1, Pallas kernels: 122 us -> 110 us  [body(): pl.pallas_call(functools.partial(kernel, nf, nt, limit, ahead), out_shape...]
    pallas_call x1, Pallas kernels: 8.36 us -> 4.21 us  [body(): pl.pallas_call(settle, out_shape=(small, small, small, small, weight, wei...]
where the time goes in v3:
time: 115 us
  Pallas kernels  114 us (99%)
    pallas_call x1, Pallas kernels, body(): pl.pallas_call(functools.partial(kernel, nf, nt, limit, ahead), out_shape...  110 us
    pallas_call x1, Pallas kernels, body(): pl.pallas_call(settle, out_shape=(small, small, small, small, weight, wei...  4.21 us

profile of v3, /device:TPU:0, one launch (start us, length us, event | category | flops | bytes accessed | tf_op | source)
XLA Modules:
  0.0 114.8 jit_solution(6787214880443861466)
XLA Ops:
  0.6 109.9 %shard_map.197 = (f32[4,24,768]{2,1,0:T(8,128)S(1)}, f32[2,192,768]{2,1,0:T(8,128)S(1)}, bf16[2,3072,768]{2,1,0:T(8,128)(2,1)S(1)}) custom-call(bf16[512,3072]{1,0:T(8,128)(2,1)} %x_hbm.1, bf16[512,3072]{1,0:T(8,128)(2,1)} %y_hbm.1, bf16[512,768]{1,0:T(8,128)(2,1)} %rec_hbm.1, bf16[512,768]{1,0:T(8,128)(2,1)} %logit_hbm.1, bf16[512,768]{1,0:T(8,128)(2,1)} %fcot_hbm.1, ...), custom_call_target="tpu_custom_call" | custom-call | tf_op jit(solution)/shard_map/pallas_call | solution.py:610
  110.6 4.2 %shard_map.198 = (f32[24,768]{1,0:T(8,128)}, f32[24,768]{1,0:T(8,128)}, f32[24,768]{1,0:T(8,128)}, f32[24,768]{1,0:T(8,128)}, f32[192,768]{1,0:T(8,128)}, /*inde...) custom-call(f32[4,24,768]{2,1,0:T(8,128)S(1)} %get-tuple-element.19.fresh, ...), custom_call_target="tpu_custom_call" | custom-call | tf_op jit(solution)/shard_map/pallas_call | solution.py:672

commit v4 on v3

--- a/solution.py
+++ b/solution.py
@@ -62,6 +62,8 @@
     part,
     peer,
     hop,
+    lead,
+    low,
     step,
     flat,
     split,
@@ -162,18 +164,16 @@
         target = lax.rem(my_id + i, everyone)
         return (target // nt, lax.rem(target, nt))
 
-    @pl.loop(1, everyone)
-    def _(i):
-        pl.semaphore_signal(barrier, inc=1, device_id=other(i), device_id_type=MESH)
-
-    pl.semaphore_wait(barrier, everyone - 1)
-
     far = n // 2
     near = n - 1 - far
     two_way = ((0, 1, far), (1, -1, far), (0, -1, near), (1, 1, near))
 
     def neighbour(way):
         return (dev_at(mod(me + way, n)), tp)
+
+    for target in (neighbour(1), neighbour(-1), partner, across):
+        pl.semaphore_signal(barrier, inc=1, device_id=target, device_id_type=MESH)
+    pl.semaphore_wait(barrier, 4)
 
     def send(src, dst, sems, target):
         return pltpu.make_async_remote_copy(
@@ -333,37 +333,58 @@
         for i in range(nf):
             part[k * 2 + i % 2, i // 2] = term[i * span : (i + 1) * span]
 
+    def place_of(j, s):
+        _, way, hops = two_way[j]
+        return chip_at(mod(me + way * (hops - s), n))
+
     def pair_sum(k):
-        sems = sum_sem.at[0, k], sum_sem.at[1, k]
-        return send(part.at[k * 2 + 1 - core], peer.at[k], sems, partner)
+        def group(s):
+            for j in (k, k + 2):
+                if not isinstance(s, int) or s < two_way[j][2] or (s == far and j == k):
+                    place = place_of(j, s)
+                    sems = sum_sem.at[0, 0], sum_sem.at[1 + k, s]
+                    send(
+                        part.at[k * 2 + 1 - core, place], peer.at[k, place], sems, partner
+                    ).start()
+
+        loop(0, near, group)
+        for s in range(near, far + 1):
+            group(s)
+
+    def paired(k, s):
+        count = 2 if not isinstance(s, int) or s < near else 1
+        arrive(peer.at[k, pl.ds(0, count)], sum_sem.at[1 + k, s])
 
     def ring_add(j, s, c):
         at = pl.ds(c * width, width)
         sems = sem_b.at[0], ring_b.at[j, s, c]
-        return send(hop.at[j, s, :, at], hop.at[j, s + 1, :, at], sems, neighbour(two_way[j][1]))
+        return send(lead.at[j, s, :, at], hop.at[j, s, :, at], sems, neighbour(two_way[j][1]))
 
     def mine(j, s, c):
-        k, way, hops = two_way[j]
+        k = two_way[j][0]
         at = pl.ds(c * width, width)
-        place = chip_at(mod(me + way * (hops - s), n))
+        place = place_of(j, s)
         return part[k * 2 + core, place, :, at] + peer[k, place, :, at]
 
     def begin(k):
-        pair_sum(k).wait_recv()
+        paired(k, 0)
         for c in range(lanes):
             at = pl.ds(c * width, width)
             for j in (k, k + 2):
                 if two_way[j][2] > 0:
-                    hop[j, 0, :, at] = mine(j, 0, c)
+                    lead[j, 0, :, at] = mine(j, 0, c).astype(lead.dtype)
                     ring_add(j, 0, c).start()
 
     def relay(j, s, c):
         at = pl.ds(c * width, width)
         ring_add(j, s - 1, c).wait_recv()
-        hop[j, s, :, at] = hop[j, s, :, at] + mine(j, s, c)
+        lead[j, s, :, at] = (hop[j, s - 1, :, at].astype(F32) + mine(j, s, c)).astype(
+            lead.dtype
+        )
         ring_add(j, s, c).start()
 
     def relay_all(k, s):
+        paired(k, s)
         for c in range(lanes):
             for j in (k, k + 2):
                 if isinstance(s, int) and s >= two_way[j][2]:
@@ -371,16 +392,17 @@
                 relay(j, s, c)
 
     def settle_sum(k):
+        paired(k, far)
         for c in range(lanes):
             at = pl.ds(c * width, width)
             ring_add(k + 2, near - 1, c).wait_recv()
-            kept = hop[k + 2, near, :, at] + mine(k + 2, near, c)
+            kept = hop[k + 2, near - 1, :, at].astype(F32) + mine(k + 2, near, c)
             ring_add(k, far - 1, c).wait_recv()
-            hop[k, far, :, at] = hop[k, far, :, at] + kept
+            low[k, :, at] = hop[k, far - 1, :, at].astype(F32) + kept
 
     late_loads[0].wait()
     project(0)
-    pair_sum(0).start()
+    pair_sum(0)
     advance()
     begin(0)
     early = max(1, near - 1)
@@ -388,7 +410,7 @@
     advance()
     arrive(coded.at[1], swap_sem.at[1])
     project(1)
-    pair_sum(1).start()
+    pair_sum(1)
     loop(early, near, lambda s: relay_all(0, s))
     begin(1)
     advance()
@@ -401,7 +423,6 @@
         relay_all(1, s)
     settle_sum(1)
 
-    low = [hop[k, far] for k in range(2)]
     square = jnp.sum(low[0] * low[0] + low[1] * low[1], axis=(0, 1), keepdims=True)
     tots[my_id] = jnp.broadcast_to(square, tots.shape[1:])
 
@@ -415,9 +436,9 @@
     advance()
 
     done_a()
-    arrive(step.at[:, pl.ds(0, n - 1)], sem_b.at[0])
-    for k in range(2):
-        pair_sum(k).wait_send()
+    arrive(lead.at[pl.ds(0, 2)], sem_b.at[0])
+    arrive(lead.at[pl.ds(0, 2), pl.ds(0, near)], sem_b.at[0])
+    arrive(peer, sum_sem.at[0, 0])
     arrive(coded.at[0], swap_sem.at[0])
     for copy in late_loads[1:7]:
         copy.wait()
@@ -434,7 +455,7 @@
     total = jnp.sum(tots[...], axis=0)
     clip = jnp.minimum(1.0, jnp.sqrt(F32(limit)) * lax.rsqrt(total + 1e-06))[0:1, 0:1]
     for t in range(2):
-        grad = clip * hop[lax.rem(q + t, 2), far]
+        grad = clip * low[lax.rem(q + t, 2)]
         moment = 0.8 * small[2 * t] + 0.2 * grad
         second = 0.9 * small[2 * t + 1] + 0.1 * grad * grad
         fresh[2 * t] = moment
@@ -623,13 +644,15 @@
             pltpu.VMEM((rank, units), F32),
             pltpu.VMEM((4, n, span, units), F32),
             pltpu.VMEM((2, n, span, units), F32),
-            pltpu.VMEM((4, far + 1, span, units), F32),
+            pltpu.VMEM((4, far, span, units), BF16),
+            pltpu.VMEM((4, far, span, units), BF16),
+            pltpu.VMEM((2, span, units), F32),
             pltpu.VMEM((2, nf, span, units), F32),
             pltpu.VMEM((rank, units), F32),
             pltpu.VMEM((2, 2 * rank, units), BF16),
             pltpu.VMEM((4, span, units), F32),
             pltpu.VMEM((2, depth, units), F32),
-            pltpu.VMEM((nf * nt, 8, 128), F32),
+            pltpu.VMEM((nf * nt, 1, 128), F32),
             pltpu.VMEM((2, n, max(ahead, 16), units), BF16),
             pltpu.VMEM((2, n * max(ahead, 16), rank), BF16),
             dma((11,)),
@@ -638,7 +661,7 @@
             dma((4, far, 1)),
             dma((1,)),
             dma((4, far, lanes)),
-            dma((2, 2)),
+            dma((3, far + 1)),
             dma((2,)),
             dma((2,)),
             dma((3,)),

time: 115 us -> 110 us (0.957)
  Pallas kernels: 114 us -> 109 us
    pallas_call x1, Pallas kernels: 110 us -> 104 us  [body(): pl.pallas_call(functools.partial(kernel, nf, nt, limit, ahead), out_shape...]
where the time goes in v4:
time: 110 us; the launch traced here: 109 us
  Pallas kernels  109 us (99%)
    pallas_call x1, Pallas kernels, body(): pl.pallas_call(functools.partial(kernel, nf, nt, limit, ahead), out_shape...  104 us
    pallas_call x1, Pallas kernels, body(): pl.pallas_call(settle, out_shape=(small, small, small, small, weight, wei...  4.21 us

profile of v4, /device:TPU:0, one launch (start us, length us, event | category | flops | bytes accessed | tf_op | source)
XLA Modules:
  0.0 109.4 jit_solution(17100087037041860189)
XLA Ops:
  0.6 104.5 %shard_map.197 = (f32[4,24,768]{2,1,0:T(8,128)S(1)}, f32[2,192,768]{2,1,0:T(8,128)S(1)}, bf16[2,3072,768]{2,1,0:T(8,128)(2,1)S(1)}) custom-call(bf16[512,3072]{1,0:T(8,128)(2,1)} %x_hbm.1, bf16[512,3072]{1,0:T(8,128)(2,1)} %y_hbm.1, bf16[512,768]{1,0:T(8,128)(2,1)} %rec_hbm.1, bf16[512,768]{1,0:T(8,128)(2,1)} %logit_hbm.1, bf16[512,768]{1,0:T(8,128)(2,1)} %fcot_hbm.1, ...), custom_call_target="tpu_custom_call" | custom-call | tf_op jit(solution)/shard_map/pallas_call | solution.py:631
  105.1 4.2 %shard_map.198 = (f32[24,768]{1,0:T(8,128)}, f32[24,768]{1,0:T(8,128)}, f32[24,768]{1,0:T(8,128)}, f32[24,768]{1,0:T(8,128)}, f32[192,768]{1,0:T(8,128)}, /*inde...) custom-call(f32[4,24,768]{2,1,0:T(8,128)S(1)} %get-tuple-element.19.fresh, ...), custom_call_target="tpu_custom_call" | custom-call | tf_op jit(solution)/shard_map/pallas_call | solution.py:695

commit v5 on v4

--- a/solution.py
+++ b/solution.py
@@ -27,6 +27,30 @@
 
 def mod(value, n):
     return lax.rem(value + 2 * n, n)
+
+
+def curve(value):
+    octave = jnp.floor(jnp.log2(value) + 1e-3)
+    return octave + value * jnp.exp2(-octave) - 1.0
+
+
+def uncurve(level):
+    octave = jnp.floor(level)
+    return (1.0 + level - octave) * jnp.exp2(octave)
+
+
+def encode(weight):
+    size = jnp.maximum(jnp.abs(weight), 2.0**-31.75)
+    index = jnp.clip(jnp.floor(1024.0 * (curve(size) + 31.75) + 0.5), 0.0, 31400.0)
+    code = uncurve(index * (1 / 128) - 120.0)
+    return jnp.where(weight < 0, -code, code).astype(BF16)
+
+
+def decode(code):
+    code = code.astype(F32)
+    level = (curve(jnp.abs(code)) + 120.0) * (1 / 8)
+    size = jnp.where(level < 1e-3, 0.0, uncurve(level - 31.75))
+    return jnp.where(code < 0, -size, size)
 
 
 def kernel(
@@ -278,7 +302,7 @@
             copy.wait()
         if ahead:
             for t in range(2):
-                pre[t, chip] = old[t, :ahead].astype(BF16)
+                pre[t, chip] = encode(old[t, :ahead])
 
     own_load.wait()
     done_a = gather(
@@ -513,27 +537,26 @@
         at = pl.multiple_of((2 * p + core) * depth, depth)
         return cp.at[t, pl.ds(at, ahead)]
 
+    pieces = []
     if ahead:
-        while at_hop[0] < n:
+        group = max(1, 192 // ahead)
+        pieces = [(k, p) for p in range(0, n, group) for k in range(2)]
+
+    def renew(k, p):
+        t = q if k == 0 else 1 - q
+        size = min(group, n - p)
+        moved = apply(lhs[k, p * ahead : (p + size) * ahead], split[t])
+        for i in range(size):
+            kept = decode(pre[t, p + i])
+            rows = rows_of(t, p + i)
+            rows[...] = (kept - 0.01 * moved[i * ahead : (i + 1) * ahead]).astype(BF16)
+            send(rows, rows, (sem_e.at[3], sem_e.at[4]), partner).start()
+
+    def some_pieces(count):
+        while at_hop[0] < n and ahead:
             advance()
-        group = max(1, 256 // ahead)
-        for k in range(2):
-            t = q if k == 0 else 1 - q
-            for p in range(0, n, group):
-                size = min(group, n - p)
-                moved = apply(lhs[k, p * ahead : (p + size) * ahead], split[t])
-                for i in range(size):
-                    kept = pre[t, p + i].astype(F32)
-                    rows_of(t, p + i)[...] = (
-                        kept - 0.01 * moved[i * ahead : (i + 1) * ahead]
-                    ).astype(BF16)
-                    send(
-                        rows_of(t, p + i),
-                        rows_of(t, p + i),
-                        (sem_e.at[3], sem_e.at[4]),
-                        partner,
-                    ).start()
-        arrive(pre, sem_e.at[4])
+        for _ in range(min(count, len(pieces))):
+            renew(*pieces.pop(0))
 
     def gone(s):
         for t in range(2):
@@ -546,9 +569,11 @@
                 pass_on(t, s - 1, c).wait_recv()
                 pass_on(t, s, c).start()
                 share(t, s, c).start()
+            some_pieces(1)
         gone(s - 1)
 
     loop(1, n - 1, forward)
+    some_pieces(len(pieces))
     for c in range(cut):
         for t in range(2):
             pass_on(t, n - 2, c).wait_recv()
@@ -559,6 +584,7 @@
     arrive(cp.at[:, pl.ds(0, (n - 1) * late)], sem_f.at[0])
     arrive(cp.at[:, pl.ds(0, n * late)], sem_f.at[1])
     if ahead:
+        arrive(pre, sem_e.at[4])
         arrive(pre, sem_e.at[3])
         arrive(pre.at[:, pl.ds(0, n - 1)], sem_e.at[0])
     done_d()
@@ -621,10 +647,10 @@
         jax.ShapeDtypeStruct((2, depth, units), F32),
         jax.ShapeDtypeStruct((2, model, units), BF16),
     )
-    cut = 2 if depth % 32 == 0 else 1
+    cut = 3 if depth % 32 == 0 else 1
     lanes = 2 if units % 256 == 0 else 1
     far = n // 2
-    ahead = depth // 3 // 16 * 16
+    ahead = depth // 2 // 16 * 16 if depth > 32 else 0
     hbm = pl.BlockSpec(memory_space=pltpu.HBM)
     vmem = pl.BlockSpec(memory_space=pltpu.VMEM)
     dma = pltpu.SemaphoreType.DMA

time: 110 us -> 107 us (0.973)
  Pallas kernels: 109 us -> 106 us
    pallas_call x1, Pallas kernels: 104 us -> 101 us  [body(): pl.pallas_call(functools.partial(kernel, nf, nt, limit, ahead), out_shape...]
where the time goes in v5:
time: 107 us; the launch traced here: 106 us
  Pallas kernels  106 us (99%)
    pallas_call x1, Pallas kernels, body(): pl.pallas_call(functools.partial(kernel, nf, nt, limit, ahead), out_shape...  101 us
    pallas_call x1, Pallas kernels, body(): pl.pallas_call(settle, out_shape=(small, small, small, small, weight, wei...  4.21 us

profile of v5, /device:TPU:0, one launch (start us, length us, event | category | flops | bytes accessed | tf_op | source)
XLA Modules:
  0.0 106.4 jit_solution(7180264436830676227)
XLA Ops:
  0.6 101.4 %shard_map.197 = (f32[4,24,768]{2,1,0:T(8,128)S(1)}, f32[2,192,768]{2,1,0:T(8,128)S(1)}, bf16[2,3072,768]{2,1,0:T(8,128)(2,1)S(1)}) custom-call(bf16[512,3072]{1,0:T(8,128)(2,1)} %x_hbm.1, bf16[512,3072]{1,0:T(8,128)(2,1)} %y_hbm.1, bf16[512,768]{1,0:T(8,128)(2,1)} %rec_hbm.1, bf16[512,768]{1,0:T(8,128)(2,1)} %logit_hbm.1, bf16[512,768]{1,0:T(8,128)(2,1)} %fcot_hbm.1, ...), custom_call_target="tpu_custom_call" | custom-call | tf_op jit(solution)/shard_map/pallas_call | solution.py:657
  102.1 4.2 %shard_map.198 = (f32[24,768]{1,0:T(8,128)}, f32[24,768]{1,0:T(8,128)}, f32[24,768]{1,0:T(8,128)}, f32[24,768]{1,0:T(8,128)}, f32[192,768]{1,0:T(8,128)}, /*inde...) custom-call(f32[4,24,768]{2,1,0:T(8,128)S(1)} %get-tuple-element.19.fresh, ...), custom_call_target="tpu_custom_call" | custom-call | tf_op jit(solution)/shard_map/pallas_call | solution.py:721

commit v6 on v5

--- a/solution.py
+++ b/solution.py
@@ -212,7 +212,7 @@
     def arrive(ref, sem):
         pltpu.make_async_copy(ref, ref, sem).wait()
 
-    def gather(view, chunks, sems, ring_sem, blocks, between=None, after=None):
+    def gather(view, chunks, sems, ring_sem, blocks, between=None, after=None, seen=None):
         flows = two_way
 
         def remote(j, s, c, pair, target):
@@ -240,17 +240,34 @@
             if not first or j < 2:
                 pair_copy(j, s, c).start()
 
+        def note(s, which):
+            if seen is not None:
+                for j in which:
+                    t, way, _ = flows[j]
+                    seen(t, dev_at(mod(me - way * s, n)))
+
         each(0, functools.partial(move, first=True))
         if between is not None:
             between()
-        loop(1, near, lambda s: each(s, move))
+        note(0, range(2))
+
+        def onward(s):
+            each(s, move)
+            note(s, range(4))
+
+        loop(1, near, onward)
         for s in range(near, far + 1):
             for c in range(chunks):
                 for j, (_, _, hops) in enumerate(flows):
                     if s <= hops:
                         move(j, s, c, last=s == hops)
+            if s < far:
+                note(s, [j for j in range(4) if s <= flows[j][2]])
         if after is not None:
             after()
+            note(far, range(2))
+        else:
+            note(far, range(2))
         arrive(blocks(n), sems.at[2])
 
         def finish():
@@ -484,7 +501,13 @@
         second = 0.9 * small[2 * t + 1] + 0.1 * grad * grad
         fresh[2 * t] = moment
         fresh[2 * t + 1] = second
-        step[t, f] = moment / (jnp.sqrt(second) + 1e-08)
+        step[t, f] = encode(moment / (jnp.sqrt(second) + 1e-08) * (1 / 32))
+
+    even = span % 8 == 0
+
+    def open_step(t, dev):
+        rows = pl.ds(pl.multiple_of(dev * span, 8), span)
+        flat[t, rows] = 32.0 * decode(step[t, dev])
 
     done_d = gather(
         lambda t, dev, c: step.at[t, dev, :, pl.ds(c * width, width)],
@@ -494,6 +517,7 @@
         lambda m: step.at[:, pl.ds(0, m)],
         None,
         advance,
+        open_step if even else None,
     )
 
     cut = ring_f.shape[2]
@@ -512,7 +536,7 @@
         sems = sem_f.at[1], pair_f.at[t, s]
         return send(block(t, s, c), block(t, s, c), sems, partner)
 
-    rank = flat.shape[0]
+    rank = flat.shape[1]
 
     def apply(mat, steps):
         return jnp.dot(
@@ -520,9 +544,13 @@
         )
 
     for t in range(2):
-        for k in range(nf):
-            flat[k * span : (k + 1) * span] = step[t, k]
-        whole = flat[...]
+        if even:
+            for p in range(n):
+                open_step(t, 2 * p + 1 - core)
+        else:
+            for k in range(nf):
+                flat[t, k * span : (k + 1) * span] = 32.0 * decode(step[t, k])
+        whole = flat[t]
         high = whole.astype(BF16)
         split[t, :rank] = high
         split[t, rank:] = (whole - high.astype(F32)).astype(BF16)
@@ -673,8 +701,8 @@
             pltpu.VMEM((4, far, span, units), BF16),
             pltpu.VMEM((4, far, span, units), BF16),
             pltpu.VMEM((2, span, units), F32),
-            pltpu.VMEM((2, nf, span, units), F32),
-            pltpu.VMEM((rank, units), F32),
+            pltpu.VMEM((2, nf, span, units), BF16),
+            pltpu.VMEM((2, rank, units), F32),
             pltpu.VMEM((2, 2 * rank, units), BF16),
             pltpu.VMEM((4, span, units), F32),
             pltpu.VMEM((2, depth, units), F32),

time: 107 us -> 104 us (0.972)
  Pallas kernels: 106 us -> 103 us
    pallas_call x1, Pallas kernels: 101 us -> 98.7 us  [body(): pl.pallas_call(functools.partial(kernel, nf, nt, limit, ahead), out_shape...]
where the time goes in v6:
time: 104 us
  Pallas kernels  103 us (99%)
    pallas_call x1, Pallas kernels, body(): pl.pallas_call(functools.partial(kernel, nf, nt, limit, ahead), out_shape...  98.7 us
    pallas_call x1, Pallas kernels, body(): pl.pallas_call(settle, out_shape=(small, small, small, small, weight, wei...  4.21 us

profile of v6, /device:TPU:0, one launch (start us, length us, event | category | flops | bytes accessed | tf_op | source)
XLA Modules:
  0.0 103.7 jit_solution(16207954855190450401)
XLA Ops:
  0.6 98.7 %shard_map.197 = (f32[4,24,768]{2,1,0:T(8,128)S(1)}, f32[2,192,768]{2,1,0:T(8,128)S(1)}, bf16[2,3072,768]{2,1,0:T(8,128)(2,1)S(1)}) custom-call(bf16[512,3072]{1,0:T(8,128)(2,1)} %x_hbm.1, bf16[512,3072]{1,0:T(8,128)(2,1)} %y_hbm.1, bf16[512,768]{1,0:T(8,128)(2,1)} %rec_hbm.1, bf16[512,768]{1,0:T(8,128)(2,1)} %logit_hbm.1, bf16[512,768]{1,0:T(8,128)(2,1)} %fcot_hbm.1, ...), custom_call_target="tpu_custom_call" | custom-call | tf_op jit(solution)/shard_map/pallas_call | solution.py:685
  99.3 4.2 %shard_map.198 = (f32[24,768]{1,0:T(8,128)}, f32[24,768]{1,0:T(8,128)}, f32[24,768]{1,0:T(8,128)}, f32[24,768]{1,0:T(8,128)}, f32[192,768]{1,0:T(8,128)}, /*inde...) custom-call(f32[4,24,768]{2,1,0:T(8,128)S(1)} %get-tuple-element.19.fresh, ...), custom_call_target="tpu_custom_call" | custom-call | tf_op jit(solution)/shard_map/pallas_call | solution.py:749

commit v7 on v6

--- a/solution.py
+++ b/solution.py
@@ -134,6 +134,7 @@
 
     depth = basis_in_hbm.shape[0]
     half = depth // 2
+    strip = half // ring_a.shape[2]
     units = cots.shape[2]
     span = part.shape[2]
     lanes = 2 if units % 256 == 0 else 1
@@ -324,9 +325,9 @@
     own_load.wait()
     done_a = gather(
         lambda t, dev, c: bas.at[
-            pl.ds(pl.multiple_of(dev * depth + t * half, half), half)
+            pl.ds(pl.multiple_of(dev * depth + t * half + c * strip, strip), strip)
         ],
-        1,
+        ring_a.shape[2],
         sem_a,
         ring_a,
         lambda m: bas.at[pl.ds(0, m * depth)],
@@ -712,7 +713,7 @@
             dma((11,)),
             dma((2,)),
             dma((3,)),
-            dma((4, far, 1)),
+            dma((4, far, 3 if depth % 96 == 0 else 1)),
             dma((1,)),
             dma((4, far, lanes)),
             dma((3, far + 1)),

time: 104 us -> 103 us (level)
  no operation moved by 1% of the time
where the time goes in v7:
time: 103 us
  Pallas kernels  102 us (99%)
    pallas_call x1, Pallas kernels, body(): pl.pallas_call(functools.partial(kernel, nf, nt, limit, ahead), out_shape...  97.7 us
    pallas_call x1, Pallas kernels, body(): pl.pallas_call(settle, out_shape=(small, small, small, small, weight, wei...  4.21 us

profile of v7, /device:TPU:0, one launch (start us, length us, event | category | flops | bytes accessed | tf_op | source)
XLA Modules:
  0.0 102.7 jit_solution(4799255793906522572)
XLA Ops:
  0.6 97.7 %shard_map.197 = (f32[4,24,768]{2,1,0:T(8,128)S(1)}, f32[2,192,768]{2,1,0:T(8,128)S(1)}, bf16[2,3072,768]{2,1,0:T(8,128)(2,1)S(1)}) custom-call(bf16[512,3072]{1,0:T(8,128)(2,1)} %x_hbm.1, bf16[512,3072]{1,0:T(8,128)(2,1)} %y_hbm.1, bf16[512,768]{1,0:T(8,128)(2,1)} %rec_hbm.1, bf16[512,768]{1,0:T(8,128)(2,1)} %logit_hbm.1, bf16[512,768]{1,0:T(8,128)(2,1)} %fcot_hbm.1, ...), custom_call_target="tpu_custom_call" | custom-call | tf_op jit(solution)/shard_map/pallas_call | solution.py:686
  98.3 4.2 %shard_map.198 = (f32[24,768]{1,0:T(8,128)}, f32[24,768]{1,0:T(8,128)}, f32[24,768]{1,0:T(8,128)}, f32[24,768]{1,0:T(8,128)}, f32[192,768]{1,0:T(8,128)}, /*inde...) custom-call(f32[4,24,768]{2,1,0:T(8,128)S(1)} %get-tuple-element.19.fresh, ...), custom_call_target="tpu_custom_call" | custom-call | tf_op jit(solution)/shard_map/pallas_call | solution.py:750
